TPU v7x, 256 devices: a whole 4x4x8 slice. The times are simulated.
256 devices in a mesh: sp: 64 (over z, x, core), tp: 4 (over y).
Axes of the slice: x: 4, y: 4, z: 8, core: 2. Of those that a mesh axis runs over, the one named last changes fastest.
Arguments:
- residual: bfloat16 [65536, 2048], P('sp'), may hold values from -6 to 6
- query: bfloat16 [65536, 1024], P('sp', 'tp'), may hold values from -6 to 6
- key: bfloat16 [65536, 256], P('sp', 'tp'), may hold values from -6 to 6
- value: bfloat16 [65536, 256], P('sp', 'tp'), may hold values from -6 to 6
- sink: float32 [16], P('tp'), may hold values from 3 to 9
- norm_gain: float32 [2048], replicated, may hold values from 0.1 to 1.9
- w_out: bfloat16 [1024, 2048], P('tp'), may hold values from -1.5 to 1.5
- w_gate: bfloat16 [2048, 4096], P('sp', 'tp'), may hold values from -0.125 to 0.125
- w_value: bfloat16 [2048, 4096], P('sp', 'tp'), may hold values from -0.125 to 0.125
- conv_gate: bfloat16 [3, 4096], P(None, 'tp'), may hold values from -3 to 3
- conv_value: bfloat16 [3, 4096], P(None, 'tp'), may hold values from -3 to 3
- w_down: bfloat16 [4096, 2048], P('tp', 'sp'), may hold values from -0.09375 to 0.09375
Outputs:
- layer_out: bfloat16 [65536, 2048], P(('sp', 'tp'))
All inputs are finite; a program needn't handle non-finite values.
Results may differ from a plain program's by a relative error of at most 0.015.
Values may be sent and summed in bfloat16 or wider, within the bound.
A program may use at most 128 MiB of HBM per device.

v0:
```python
import jax
import jax.numpy as jnp
from jax import lax
from jax.sharding import PartitionSpec as P

HD = 64
WINDOW = 128


THETA = 10000.0
EPS = 1e-06


def turned_gather(arrays, axis, dims):
    turned = [jnp.moveaxis(a, dim, 0) for a, dim in zip(arrays, dims)]
    both = jnp.concatenate([t.reshape(len(t), -1) for t in turned], axis=1)
    filled, at, finished = (lax.all_gather(both, axis, axis=0, tiled=True), 0, [])
    for t, dim in zip(turned, dims):
        share = filled[:, at : at + t[0].size].reshape(-1, *t.shape[1:])
        finished.append(jnp.moveaxis(share, 0, dim))
        at += t[0].size
    return tuple(finished)


def extended(block, sides, width):
    for axis, dim in sides:
        count = lax.axis_size(axis)
        forward = [(i, i + 1) for i in range(count - 1)]
        backward = [(target, source) for source, target in forward]
        low = lax.ppermute(
            lax.slice_in_dim(block, block.shape[dim] - width, None, axis=dim), axis, forward
        )
        high = lax.ppermute(lax.slice_in_dim(block, 0, width, axis=dim), axis, backward)
        block = jnp.concatenate([low, block, high], axis=dim)
    return block


def in_blocks(shard, dim, devices):
    shape = shard.shape
    tiles = shard.reshape(*shape[:dim], devices, shape[dim] // devices, *shape[dim + 1 :])
    return jnp.moveaxis(tiles, dim, 0)


def summed_on_arrival(shard, axis, dim):
    tiles = in_blocks(shard, dim, lax.axis_size(axis))
    arrived = lax.all_to_all(tiles, axis, split_axis=0, concat_axis=0, tiled=True)
    return arrived.astype(jnp.float32).sum(axis=0)


def rotate(field, positions):
    count = field.shape[0]
    parts = field.astype(jnp.float32).reshape(count, -1, HD)
    inverse = 1.0 / THETA ** (jnp.arange(0, HD, 2, dtype=jnp.float32) / HD)
    angle = positions[:, None] * inverse[None, :]
    cosine = jnp.cos(angle)[:, None, :]
    sine = jnp.sin(angle)[:, None, :]
    first = parts[..., : HD // 2]
    second = parts[..., HD // 2 :]
    turned = jnp.concatenate(
        [first * cosine - second * sine, second * cosine + first * sine], axis=-1
    )
    return turned.reshape(count, -1).astype(jnp.bfloat16)


def band_attention(queries, keys, values, sinks, start, total):
    count = queries.shape[0]
    blocks = count // WINDOW
    kv_local = keys.shape[1] // HD
    group = queries.shape[1] // (kv_local * HD)
    query_blocks = queries.reshape(blocks, WINDOW, kv_local, group, HD)
    key_band = jnp.concatenate(
        [
            keys[i * WINDOW : i * WINDOW + count].reshape(blocks, WINDOW, kv_local, HD)
            for i in range(3)
        ],
        axis=1,
    )
    value_band = jnp.concatenate(
        [
            values[i * WINDOW : i * WINDOW + count].reshape(blocks, WINDOW, kv_local, HD)
            for i in range(3)
        ],
        axis=1,
    )
    scores = jnp.einsum(
        "nqkgd,njkd->nkgqj", query_blocks, key_band, preferred_element_type=jnp.float32
    ) * HD ** (-0.5)
    block_ids = jnp.arange(blocks, dtype=jnp.int32)[:, None]
    query_pos = start + block_ids * WINDOW + jnp.arange(WINDOW, dtype=jnp.int32)[None, :]
    key_pos = start - WINDOW + block_ids * WINDOW + jnp.arange(3 * WINDOW, dtype=jnp.int32)[None, :]
    valid = (
        (key_pos[:, None, :] >= 0)
        & (key_pos[:, None, :] < total)
        & (jnp.abs(query_pos[:, :, None] - key_pos[:, None, :]) <= WINDOW)
    )
    scores = jnp.where(valid[:, None, None], scores, -1e30)
    sink_col = sinks.reshape(1, kv_local, group, 1, 1)
    top = jnp.maximum(jnp.max(scores, axis=-1, keepdims=True), sink_col)
    weights = jnp.exp(scores - top)
    denom = jnp.sum(weights, axis=-1, keepdims=True) + jnp.exp(sink_col - top)
    probs = (weights / denom).astype(jnp.bfloat16)
    out = jnp.einsum("nkgqj,njkd->nqkgd", probs, value_band, preferred_element_type=jnp.float32)
    return out.reshape(count, kv_local * group * HD).astype(jnp.bfloat16)


def rmsnorm(field, gain):
    wide = field.astype(jnp.float32)
    scale = lax.rsqrt(jnp.mean(wide * wide, axis=-1, keepdims=True) + EPS)
    return (wide * scale * gain).astype(jnp.bfloat16)


def shards(
    residual,
    query,
    key,
    value,
    sink,
    norm_gain,
    w_out,
    w_gate,
    w_value,
    conv_gate,
    conv_value,
    w_down,
):
    tok_rows = query.shape[0]
    offset = lax.axis_index("sp") * tok_rows
    total = tok_rows * lax.axis_size("sp")
    share = tok_rows // lax.axis_size("tp")
    tp_index = lax.axis_index("tp")
    gate_full, value_full, down_full = turned_gather((w_gate, w_value, w_down), "sp", (0, 0, 1))
    positions = (offset + jnp.arange(tok_rows, dtype=jnp.int32)).astype(jnp.float32)
    turned_query = rotate(query, positions)
    turned_key = rotate(key, positions)
    key_width = key.shape[1]
    band = jnp.concatenate([turned_key, value], axis=1)
    edged = extended(band, (("sp", 0),), WINDOW)
    attended = band_attention(
        turned_query, edged[:, :key_width], edged[:, key_width:], sink, offset, total
    )
    partial_value = jnp.dot(attended, w_out, preferred_element_type=jnp.float32)
    mix_full = lax.psum(partial_value.astype(jnp.bfloat16), "tp").astype(jnp.float32)
    mid_full = (residual.astype(jnp.float32) + mix_full).astype(jnp.bfloat16)
    normed = rmsnorm(mid_full, norm_gain)
    mid_rows = lax.dynamic_slice_in_dim(mid_full, tp_index * share, share, 0)
    gate_up = jnp.dot(normed, gate_full, preferred_element_type=jnp.float32).astype(jnp.bfloat16)
    value_up = jnp.dot(normed, value_full, preferred_element_type=jnp.float32).astype(jnp.bfloat16)
    hidden_width = gate_up.shape[1]
    stacked = jnp.concatenate([gate_up, value_up], axis=1)
    edged_up = extended(stacked, (("sp", 0),), 1).astype(jnp.float32)
    taps = jnp.concatenate([conv_gate, conv_value], axis=1).astype(jnp.float32)
    convolved = edged_up[:-2] * taps[0] + edged_up[1:-1] * taps[1] + edged_up[2:] * taps[2]
    hidden = (jax.nn.silu(convolved[:, :hidden_width]) * convolved[:, hidden_width:]).astype(
        jnp.bfloat16
    )
    terms = jnp.dot(hidden, down_full, preferred_element_type=jnp.float32)
    ffn_rows = summed_on_arrival(terms.astype(jnp.bfloat16), "tp", 0)
    return (mid_rows.astype(jnp.float32) + ffn_rows).astype(jnp.bfloat16)


def solution(mesh):
    return jax.shard_map(
        shards,
        mesh=mesh,
        in_specs=(
            P("sp", None),
            P("sp", "tp"),
            P("sp", "tp"),
            P("sp", "tp"),
            P("tp"),
            P(),
            P("tp", None),
            P("sp", "tp"),
            P("sp", "tp"),
            P(None, "tp"),
            P(None, "tp"),
            P("tp", "sp"),
        ),
        out_specs=P(("sp", "tp"), None),
        check_vma=False,
    )
```

profile of v0, /device:TPU:7, one launch (start us, length us, event | category | flops | bytes accessed | tf_op | source)
XLA Modules:
  0.0 262.5 jit_solution(6383390752943163)
XLA Ops:
  7.4 0.0 copy-start
  7.4 0.0 all-reduce.2.cloned.1.call-start
  7.4 1.0 bitcast_convert_fusion
  8.4 0.6 fusion.55
  9.0 0.7 pad_maximum_fusion.7
  9.8 4.0 %collective-permute-start = (bf16[128,128]{0,1:T(8,128)(2,1)S(1)}, bf16[128,128]{0,1:T(8,128)(2,1)S(1)}, u32[]{:S(2)}, u32[]{:S(2)}) collective-permute-start(bf16[128,128]{0,1:T(8,128)(2,1)S(1)} %get-tuple-element.19), channel_id=1, source_target_pairs={{0,4},{4,8},{8,12},{12,16},{16,20},{20,24},{24,28},{28,32},{32,36}... | collective-permute-start | bytes 98312 | tf_op jit(solution)/shard_map/ppermute | solution.py:30
  13.8 1.9 collective-permute-start.1
  15.8 0.1 compare_and_fusion
  15.8 0.1 iota_add_fusion
  15.9 0.5 multiply_cosine_fusion
  16.4 0.1 iota_add_fusion.1
  16.5 1.2 copy.20
  17.8 0.1 convert.11
  17.9 0.1 subtract_convert_fusion
  18.0 1.2 fusion.27
  19.2 0.0 copy-done.3
  19.3 0.0 collective-permute-done
  19.3 1.8 collective-permute-done.1
  21.2 0.1 maximum_bitcast_fusion.6
  21.5 0.0 copy-start.9
  21.5 1.1 fusion.6
  22.5 0.0 copy-done.9
  22.5 0.1 broadcast_maximum_fusion
  22.6 1.5 fusion.5
  24.1 0.1 exponential_add_fusion
  24.2 1.9 fusion.31
  26.1 0.3 copy.23
  26.5 0.0 copy-done
  26.5 0.0 copy-start.4
  26.5 0.0 copy-start.5
  26.5 0.0 copy-start.6
  26.5 3.2 %convolution_convert_fusion = bf16[1024,2048]{1,0:T(8,128)(2,1)} fusion(bf16[256,2048]{1,0:T(8,128)(2,1)S(1)} %copy-done, bf16[32,8,8,128]{3,2,1,0:T(8,128)(2,1)S(1)} %bitcast.106), kind=kOutput, calls=%fused_computation.30 | convolution fusion | flops 1075838976 | bytes 5767168 | tf_op jit(solution)/shard_map/dot_general | solution.py:141
  29.8 0.0 all-reduce.2.cloned.1.call-update
  29.8 0.2 all-gather.2.cloned.1.call-start
  30.1 0.0 copy-done.4
  30.1 0.0 copy-done.5
  30.1 0.0 copy-done.6
  30.1 0.7 pad_maximum_fusion.1
  30.8 0.0 all-gather.2.cloned.1.call-update
  30.8 0.0 copy-done.7
  30.8 0.0 copy-done.8
  30.8 0.0 copy-start.10
  30.9 98.8 %all-reduce.2.cloned.1.call-done = bf16[1024,2048]{1,0:T(8,128)(2,1)} async-done(((bf16[1024,2048]{1,0:T(8,128)(2,1)}), bf16[1024,2048]{1,0:T(8,128)(2,1)}) %all-reduce.2.cloned.1.call-update) | async-done | bytes 4194320 | tf_op jit(solution)/shard_map/psum | solution.py:142
  129.7 7.4 %fusion = (f32[1024]{0:T(1024)S(1)}, bf16[1024,2048]{1,0:T(8,128)(2,1)}) fusion(bf16[1024,2048]{1,0:T(8,128)(2,1)} %all-reduce.2.cloned.1.call-done, bf16[1024,2048]{1,0:T(8,128)(2,1)} %param.12), kind=kLoop, calls=%fused_computation.2 | loop fusion | flops 14679040 | bytes 12587008 | tf_op jit(solution)/shard_map/reduce_sum | solution.py:108
  137.1 0.0 copy-done.10
  137.1 0.0 copy-start.2
  137.1 8.5 %fusion.24 = bf16[1024,1024]{0,1:T(8,128)(2,1)S(1)} fusion(bf16[2048,3072]{1,0:T(8,128)(2,1)} %all-gather.2.cloned.1.call-done, bf16[1024,2048]{1,0:T(8,128)(2,1)} %get-tuple-element.6, f32[2048]{0:T(1024)S(1)} %copy-done.10, f32[1024]{0:T(1024)S(1)} %add_rsqrt_fusion), kind=kOutput, calls=%fused_computation.37 | convolution fusion | flops 4304404480 | bytes 10498048 | tf_op jit(solution)/shard_map/dot_general | solution.py:147
  145.7 0.0 copy-done.2
  145.7 7.5 %fusion.21 = bf16[1024,1024]{0,1:T(8,128)(2,1)S(1)} fusion(bf16[2048,3072]{1,0:T(8,128)(2,1)} %all-gather.2.cloned.1.call-done, bf16[1024,2048]{1,0:T(8,128)(2,1)S(1)} %copy-done.2, f32[2048]{0:T(1024)S(1)} %copy-done.10, f32[1024]{0:T(1024)S(1)} %add_rsqrt_fusion), kind=kOutput, calls=%fused_computation.36 | convolution fusion | flops 4304404480 | bytes 10498048 | tf_op jit(solution)/shard_map/dot_general | solution.py:146
  153.2 0.3 fusion.37
  153.5 2.7 %collective-permute-start.3 = (bf16[1,2048]{0,1:T(8,128)(2,1)S(1)}, bf16[1,2048]{0,1:T(8,128)(2,1)S(1)}, u32[]{:S(2)}, u32[]{:S(2)}) collective-permute-start(bf16[1,2048]{0,1:T(8,128)(2,1)S(1)} %get-tuple-element.7), channel_id=1, source_target_pairs={{4,0},{8,4},{12,8},{16,12},{20,16},{24,20},{28,24},{32,28},{36,32}... | collective-permute-start | bytes 12296 | tf_op jit(solution)/shard_map/ppermute | solution.py:33
  156.2 5.1 %collective-permute-start.2 = (bf16[1,2048]{0,1:T(8,128)(2,1)S(1)}, bf16[1,2048]{0,1:T(8,128)(2,1)S(1)}, u32[]{:S(2)}, u32[]{:S(2)}) collective-permute-start(bf16[1,2048]{0,1:T(8,128)(2,1)S(1)} %get-tuple-element.8), channel_id=1, source_target_pairs={{0,4},{4,8},{8,12},{12,16},{16,20},{20,24},{24,28},{28,32},{32,36}... | collective-permute-start | bytes 12296 | tf_op jit(solution)/shard_map/ppermute | solution.py:30
  161.4 2.5 pad_maximum_fusion
  163.9 2.2 collective-permute-done.3
  166.1 1.2 collective-permute-done.2
  167.3 9.3 %concatenate.46 = bf16[1026,2048]{0,1:T(8,128)(2,1)} concatenate(bf16[1,2048]{0,1:T(8,128)(2,1)S(1)} %collective-permute-done.2, bf16[1024,2048]{0,1:T(8,128)(2,1)} %pad_maximum_fusion, bf16[1,2048]{0,1:T(8,128)(2,1)S(1)} %collective-permute-done.3), dimensions={0} | concatenate | bytes 8404992 | tf_op jit(solution)/shard_map/concatenate | solution.py:34
  176.6 2.9 %convert_element_type.108 = f32[1026,2048]{0,1:T(8,128)S(1)} convert(bf16[1026,2048]{0,1:T(8,128)(2,1)} %concatenate.46) | non-fusion elementwise | flops 2101248 | bytes 12607488 | tf_op jit(solution)/shard_map/convert_element_type | solution.py:150
  179.5 6.9 %fusion.3 = f32[1024,2048]{0,1:T(8,128)S(1)} fusion(f32[1026,2048]{0,1:T(8,128)S(1)} %convert_element_type.108, f32[2048]{0:T(1024)S(1)} %bitcast.118, f32[2048]{0:T(1024)S(1)} %bitcast.117, f32[2048]{0:T(1024)S(1)} %bitcast.116), kind=kLoop, calls=%fused_computation.6 | loop fusion | flops 10485760 | bytes 33579008 | tf_op jit(solution)/shard_map/add | solution.py:152
  186.5 8.5 %fusion.14 = bf16[1024,2048]{1,0:T(8,128)(2,1)} fusion(bf16[2048,3072]{1,0:T(8,128)(2,1)} %all-gather.2.cloned.1.call-done, f32[1024,2048]{0,1:T(8,128)S(1)} %fusion.3), kind=kOutput, calls=%fused_computation.31 | convolution fusion | flops 4303355904 | bytes 16777216 | tf_op jit(solution)/shard_map/dot_general | solution.py:156
  195.0 4.8 %all-to-all-start = ((bf16[4,256,2048]{2,1,0:T(8,128)(2,1)}), bf16[4,256,2048]{2,1,0:T(8,128)(2,1)}, u32[]{:S(2)}, u32[]{:S(2)}) async-start(bf16[4,256,2048]{2,1,0:T(8,128)(2,1)} %bitcast.105), calls=%async_computation | async-start | bytes 8388608 | tf_op jit(solution)/shard_map/all_to_all | solution.py:46
  199.9 0.0 copy-start.1
  199.9 49.4 %all-to-all-done = bf16[4,256,2048]{2,1,0:T(8,128)(2,1)} async-done(((bf16[4,256,2048]{2,1,0:T(8,128)(2,1)}), bf16[4,256,2048]{2,1,0:T(8,128)(2,1)}, u32[]{:S(2)}, u32[]{:S(2)}) %all-to-all-start) | async-done | bytes 4194336 | tf_op jit(solution)/shard_map/all_to_all | solution.py:46
  249.3 3.3 %convert_reduce_fusion = f32[256,2048]{1,0:T(8,128)S(1)} fusion(bf16[4,256,2048]{2,1,0:T(8,128)(2,1)} %all-to-all-done), kind=kLoop, calls=%fused_computation.10 | loop fusion | flops 3670016 | bytes 6291456 | tf_op jit(solution)/shard_map/reduce_sum | solution.py:47
  252.5 2.5 add_convert_fusion.1
  (23 shorter events, 0.3 us)
Async XLA Ops:
  7.4 19.1 %copy-start = (bf16[256,2048]{1,0:T(8,128)(2,1)S(1)}, bf16[256,2048]{1,0:T(8,128)(2,1)}, u32[]{:S(2)}) copy-start(bf16[256,2048]{1,0:T(8,128)(2,1)} %param.18) | copy-start | bytes 3145732
  7.4 11.8 %copy-start.3 = (bf16[1024,64]{0,1:T(8,128)(2,1)S(1)}, bf16[1024,64]{0,1:T(8,128)(2,1)}, u32[]{:S(2)}) copy-start(bf16[1024,64]{0,1:T(8,128)(2,1)} %param.15) | copy-start | bytes 393220
  7.4 122.3 %all-reduce.2.cloned.1.call-start = ((), (), s32[]{:S(2)}) async-start(), calls=%async_computation.1 | async-start | bytes 8388608 | tf_op jit(solution)/shard_map/psum | solution.py:142
  9.8 9.5 %collective-permute-start = (bf16[128,128]{0,1:T(8,128)(2,1)S(1)}, bf16[128,128]{0,1:T(8,128)(2,1)S(1)}, u32[]{:S(2)}, u32[]{:S(2)}) collective-permute-start(bf16[128,128]{0,1:T(8,128)(2,1)S(1)} %get-tuple-element.19), channel_id=1, source_target_pairs={{0,4},{4,8},{8,12},{12,16},{16,20},{20,24},{24,28},{28,32},{32,36}... | collective-permute-start | bytes 98312 | tf_op jit(solution)/shard_map/ppermute | solution.py:30
  13.8 7.3 %collective-permute-start.1 = (bf16[128,128]{0,1:T(8,128)(2,1)S(1)}, bf16[128,128]{0,1:T(8,128)(2,1)S(1)}, u32[]{:S(2)}, u32[]{:S(2)}) collective-permute-start(bf16[128,128]{0,1:T(8,128)(2,1)S(1)} %get-tuple-element.20), channel_id=1, source_target_pairs={{4,0},{8,4},{12,8},{16,12},{20,16},{24,20},{28,24},{32,28},{36,32}... | collective-permute-start | bytes 98312 | tf_op jit(solution)/shard_map/ppermute | solution.py:33
  21.5 1.1 copy-start.9
  26.5 3.5 %copy-start.4 = (bf16[1024,32]{0,1:T(8,128)(2,1)S(1)}, bf16[1024,32]{0,1:T(8,128)(2,1)}, u32[]{:S(2)}) copy-start(bf16[1024,32]{0,1:T(8,128)(2,1)} %param.23) | copy-start | bytes 196612
  26.5 3.5 %copy-start.5 = (bf16[32,1024]{1,0:T(8,128)(2,1)S(1)}, bf16[32,1024]{1,0:T(8,128)(2,1)}, u32[]{:S(2)}) copy-start(bf16[32,1024]{1,0:T(8,128)(2,1)} %param.20) | copy-start | bytes 196612
  26.5 3.5 %copy-start.6 = (bf16[32,1024]{1,0:T(8,128)(2,1)S(1)}, bf16[32,1024]{1,0:T(8,128)(2,1)}, u32[]{:S(2)}) copy-start(bf16[32,1024]{1,0:T(8,128)(2,1)} %param.19) | copy-start | bytes 196612
  29.8 1.0 copy-start.7
  29.8 1.0 copy-start.8
  29.8 107.3 %all-gather.2.cloned.1.call-start = ((), (), s32[]{:S(2)}) async-start(), calls=%async_computation.2 | async-start | bytes 12779520 | tf_op jit(solution)/shard_map/all_gather | solution.py:17
  30.8 106.3 %copy-start.10 = (f32[2048]{0:T(1024)S(1)}, f32[2048]{0:T(1024)}, u32[]{:S(2)}) copy-start(f32[2048]{0:T(1024)} %param.17) | copy-start | bytes 24580
  137.1 8.5 %copy-start.2 = (bf16[1024,2048]{1,0:T(8,128)(2,1)S(1)}, bf16[1024,2048]{1,0:T(8,128)(2,1)}, u32[]{:S(2)}) copy-start(bf16[1024,2048]{1,0:T(8,128)(2,1)} %get-tuple-element.6) | copy-start | bytes 12582916
  153.5 12.6 %collective-permute-start.3 = (bf16[1,2048]{0,1:T(8,128)(2,1)S(1)}, bf16[1,2048]{0,1:T(8,128)(2,1)S(1)}, u32[]{:S(2)}, u32[]{:S(2)}) collective-permute-start(bf16[1,2048]{0,1:T(8,128)(2,1)S(1)} %get-tuple-element.7), channel_id=1, source_target_pairs={{4,0},{8,4},{12,8},{16,12},{20,16},{24,20},{28,24},{32,28},{36,32}... | collective-permute-start | bytes 12296 | tf_op jit(solution)/shard_map/ppermute | solution.py:33
  156.2 11.0 %collective-permute-start.2 = (bf16[1,2048]{0,1:T(8,128)(2,1)S(1)}, bf16[1,2048]{0,1:T(8,128)(2,1)S(1)}, u32[]{:S(2)}, u32[]{:S(2)}) collective-permute-start(bf16[1,2048]{0,1:T(8,128)(2,1)S(1)} %get-tuple-element.8), channel_id=1, source_target_pairs={{0,4},{4,8},{8,12},{12,16},{16,20},{20,24},{24,28},{28,32},{32,36}... | collective-permute-start | bytes 12296 | tf_op jit(solution)/shard_map/ppermute | solution.py:30
  195.0 54.2 %all-to-all-start = ((bf16[4,256,2048]{2,1,0:T(8,128)(2,1)}), bf16[4,256,2048]{2,1,0:T(8,128)(2,1)}, u32[]{:S(2)}, u32[]{:S(2)}) async-start(bf16[4,256,2048]{2,1,0:T(8,128)(2,1)} %bitcast.105), calls=%async_computation | async-start | bytes 8388608 | tf_op jit(solution)/shard_map/all_to_all | solution.py:46
  199.9 55.2 %copy-start.1 = (bf16[256,2048]{1,0:T(8,128)(2,1)S(1)}, bf16[256,2048]{1,0:T(8,128)(2,1)}, u32[]{:S(2)}) copy-start(bf16[256,2048]{1,0:T(8,128)(2,1)} %param.18) | copy-start | bytes 3145732
Sparse Core Ops, SparseCore 0:
  29.9 99.7 all-reduce.1
Sparse Core Ops, SparseCore 1:
  33.1 89.9 all-gather.1
where the time goes:
time: 263 us; the launch traced here: 262 us
  waiting for transfers between devices  153 us (58%)
  other arithmetic  32.8 us (12%)
  matrix products  30.8 us (12%)
  starting transfers between devices  18.9 us (7%)
  between operations  15.3 us (6%)
  local copies, waits for them, and re-layouts  11.2 us (4%)
    psum x1, waiting for transfers between devices, shards(): lax.psum(partial_value.astype(jnp.bfloat16), 'tp').astype(jnp.float32)  98.8 us
    all_to_all x1, waiting for transfers between devices, summed_on_arrival(): lax.all_to_all(tiles, axis, split_axis=0, concat_axis=0, tiled=True)  49.4 us
    concatenate x1, local copies, waits for them, and re-layouts, extended(): block = jnp.concatenate([low, block, high], axis=dim)  9.32 us
    ppermute x2, starting transfers between devices, extended(): lax.ppermute(lax.slice_in_dim(block, block.shape[dim] - width, None, axis...  9.16 us
    dot_general x1, matrix products, shards(): terms = jnp.dot(hidden, down_full, preferred_element_type=jnp.float32)  8.53 us
    dot_general x1, matrix products, shards(): jnp.dot(normed, value_full, preferred_element_type=jnp.float32)  8.53 us
    dot_general x1, matrix products, shards(): jnp.dot(normed, gate_full, preferred_element_type=jnp.float32)  7.53 us
    reduce_sum x1, other arithmetic, rmsnorm(): scale = lax.rsqrt(jnp.mean(wide * wide, axis=-1, keepdims=True) + EPS)  7.4 us
  transfers between devices with their start and end apart: 7, of which 5 were waited for; matrix products, arithmetic and copies ran while one was open for 5% of the time, Pallas kernels for 0%

commit v1 on v0

v1 whole, which is shorter than its diff:
```python
import functools

import jax
import jax.numpy as jnp
from jax import lax
from jax.experimental import pallas as pl
from jax.experimental.pallas import tpu as pltpu
from jax.sharding import PartitionSpec as P

HD = 64
WINDOW = 128
THETA = 10000.0
EPS = 1e-06
MESH = pl.DeviceIdType.MESH

NZ, NX, NC, NY = 8, 4, 2, 4
ROWS = 1024
D = 2048
FL = 1024
QC = 256
CH = 256
HALO = 16
NSEM = 112
NLOC = 8
NT = (((1,), (1,)), ((), ()))
F32 = jnp.float32
BF16 = jnp.bfloat16


class Comm:
    def __init__(self, send, recv, local):
        self.send, self.recv, self.local = send, recv, local
        self.count, self.lcount = 0, 0
        self.all = []

    def start(self, src, dst, **where):
        k = self.count
        self.count += 1
        copy = pltpu.make_async_remote_copy(
            src_ref=src,
            dst_ref=dst,
            send_sem=self.send.at[k],
            recv_sem=self.recv.at[k],
            device_id=where,
            device_id_type=MESH,
        )
        copy.start()
        self.all.append(copy)
        return copy

    def here(self, src, dst):
        copy = pltpu.make_async_copy(src, dst, self.local.at[self.lcount])
        self.lcount += 1
        copy.start()
        return copy


def turned(x, cosine, sine):
    lane = lax.broadcasted_iota(jnp.int32, x.shape, 1)
    other = jnp.where((lane & 63) < 32, pltpu.roll(x, 96, 1), pltpu.roll(x, 32, 1))
    return x * cosine + other * sine


def layer(
    sink_ref,
    q_ref,
    kv_ref,
    cos_ref,
    sin_ref,
    gain_ref,
    taps_ref,
    res_hbm,
    wo_hbm,
    g_hbm,
    vd_hbm,
    out_ref,
    kvx,
    qr,
    ka,
    kb,
    va,
    vb,
    att,
    wo,
    res,
    nrm,
    edge,
    g,
    vd,
    hid,
    part,
    own,
    rin,
    fin,
    send,
    recv,
    local,
):
    s = lax.axis_index("sp")
    t = lax.axis_index("tp")
    nsp = NZ * NX * NC
    z, x, c = s // (NX * NC), (s // NC) % NX, s % NC

    def at(dz, dx, dc=0):
        return (((z + dz + NZ) % NZ) * NX + (x + dx + NX) % NX) * NC + (c + dc) % NC

    def zi(dz):
        return (z + dz + NZ) % NZ

    def xi(dx):
        return (x + dx + NX) % NX

    ahead, behind = (s + 1) % nsp, (s + nsp - 1) % nsp
    mate = at(0, 0, 1)
    ty = [(t + k) % NY for k in range(NY)]

    barrier = pltpu.get_barrier_semaphore()
    peers = [{"sp": i} for i in (ahead, behind, at(1, 0), at(-1, 0), at(0, 1), at(0, 2), at(0, 3), mate)]
    peers += [{"tp": ty[k]} for k in (1, 2, 3)]
    for peer in peers:
        pl.semaphore_signal(barrier, inc=1, device_id=peer, device_id_type=MESH)
    pl.semaphore_wait(barrier, len(peers))

    cm = Comm(send, recv, local)

    h_low = cm.start(kv_ref.at[pl.ds(ROWS - WINDOW, WINDOW)], kvx.at[pl.ds(0, WINDOW)], sp=ahead)
    h_high = cm.start(kv_ref.at[pl.ds(0, WINDOW)], kvx.at[pl.ds(WINDOW + ROWS, WINDOW)], sp=behind)
    l_kv = cm.here(kv_ref, kvx.at[pl.ds(WINDOW, ROWS)])

    def vcell(dz, dx=0):
        return vd.at[zi(dz), xi(dx), c]

    def grow(dz):
        return g.at[zi(dz), :, c]

    vright = {0: cm.start(vd_hbm, vcell(0), sp=at(1, 0))}
    vleft = {0: cm.start(vd_hbm, vcell(0), sp=at(-1, 0))}
    g_x = [cm.start(g_hbm, g.at[z, x, c], sp=at(0, k)) for k in (1, 2, 3)]
    vx = {0: (cm.start(vd_hbm, vcell(0), sp=at(0, 1)), cm.start(vd_hbm, vcell(0), sp=at(0, -1)))}
    half = pl.ds(pl.multiple_of(c * 128, 128), 128)
    worow = pl.ds(pl.multiple_of(t * QC + c * 128, 128), 128)
    wo_y = [cm.start(wo_hbm.at[half], wo.at[worow], tp=ty[k]) for k in (1, 3, 2)]
    v_push = [cm.start(vd_hbm, vcell(0), sp=mate)]
    l_g = cm.here(g_hbm, g.at[z, x, c])
    l_v = cm.here(vd_hbm, vcell(0))
    l_wo = cm.here(wo_hbm, wo.at[pl.ds(pl.multiple_of(t * QC, QC), QC)])
    l_res = cm.here(res_hbm, res)

    @pl.loop(0, ROWS // WINDOW)
    def _(b):
        rows = pl.ds(pl.multiple_of(b * WINDOW, WINDOW), WINDOW)
        trows = pl.ds(pl.multiple_of(b * WINDOW + WINDOW, WINDOW), WINDOW)
        for p in range(2):
            lanes = slice(p * 128, p * 128 + 128)
            qr[rows, lanes] = turned(
                q_ref[rows, lanes].astype(F32), cos_ref[trows, :], sin_ref[trows, :]
            ).astype(BF16)

    l_kv.wait()
    h_low.wait_recv()
    h_high.wait_recv()

    @pl.loop(0, ROWS // WINDOW + 2)
    def _(b):
        rows = pl.ds(pl.multiple_of(b * WINDOW, WINDOW), WINDOW)
        both = kvx[rows, :].astype(F32)
        lane = lax.broadcasted_iota(jnp.int32, both.shape, 1)
        keys = jnp.where(lane < HD, turned(both, cos_ref[rows, :], sin_ref[rows, :]), 0.0)
        values = jnp.where(lane < HD, 0.0, both)
        ka[rows, :] = keys.astype(BF16)
        kb[rows, :] = pltpu.roll(keys, HD, 1).astype(BF16)
        va[rows, :] = pltpu.roll(values, HD, 1).astype(BF16)
        vb[rows, :] = values.astype(BF16)

    def attend(b):
        start = pl.multiple_of(b * WINDOW, WINDOW)
        rows = pl.ds(start, WINDOW)
        band = pl.ds(start, 3 * WINDOW)
        r = lax.broadcasted_iota(jnp.int32, (WINDOW, 3 * WINDOW), 0)
        j = lax.broadcasted_iota(jnp.int32, (WINDOW, 3 * WINDOW), 1)
        first = s * ROWS + start - WINDOW
        valid = (j >= r) & (j <= r + 2 * WINDOW) & (j + first >= 0) & (j + first < nsp * ROWS)
        lane = lax.broadcasted_iota(jnp.int32, (WINDOW, 128), 1)
        vv = jnp.concatenate([va[band, :], vb[band, :]], axis=0)
        for p in range(2):
            qp = qr[rows, p * 128 : p * 128 + 128]
            weights, inverse = [], []
            for i, keys in enumerate((ka, kb)):
                sc = lax.dot_general(qp, keys[band, :], NT, preferred_element_type=F32)
                sc = jnp.where(valid, sc * HD ** (-0.5), -1e30)
                sink = sink_ref[2 * p + i]
                top = jnp.maximum(jnp.max(sc, axis=1, keepdims=True), sink)
                w = jnp.exp(sc - top)
                denom = jnp.sum(w, axis=1, keepdims=True) + jnp.exp(sink - top)
                weights.append(w.astype(BF16))
                inverse.append(1.0 / denom)
            o = jnp.dot(jnp.concatenate(weights, axis=1), vv, preferred_element_type=F32)
            o = o * jnp.where(lane < HD, inverse[0], inverse[1])
            att[rows, pl.ds(pl.multiple_of(t * QC + p * 128, 128), 128)] = o.astype(BF16)

    def attend_chunk(ci):
        @pl.loop(0, 2)
        def _(i):
            attend(ci * 2 + i)

    a_y = {}

    def send_att(ci):
        piece = att.at[pl.ds(ci * CH, CH), pl.ds(pl.multiple_of(t * QC, QC), QC)]
        a_y[ci] = [cm.start(piece, piece, tp=ty[k]) for k in (1, 3, 2)]

    gright, gleft, g_push, vfwd, v_cols = {}, {}, [], {}, []

    def g_first():
        l_g.wait()
        for copy in g_x:
            copy.wait_recv()
        gright[0] = cm.start(grow(0), grow(0), sp=at(1, 0))
        gleft[0] = cm.start(grow(0), grow(0), sp=at(-1, 0))
        g_push.append(cm.start(grow(0), grow(0), sp=mate))

    def v_round(k):
        vright[k - 1].wait_recv()
        cell = vcell(-k)
        if k < 4:
            vright[k] = cm.start(cell, cell, sp=at(1, 0))
        vx[-k] = (cm.start(cell, cell, sp=at(0, 1)), cm.start(cell, cell, sp=at(0, -1)))
        v_push.append(cm.start(cell, cell, sp=mate))
        if k < 4:
            vleft[k - 1].wait_recv()
            cell = vcell(k)
            if k < 3:
                vleft[k] = cm.start(cell, cell, sp=at(-1, 0))
            vx[k] = (cm.start(cell, cell, sp=at(0, 1)), cm.start(cell, cell, sp=at(0, -1)))
            v_push.append(cm.start(cell, cell, sp=mate))

    def v_across(o):
        vx[o][0].wait_recv()
        vx[o][1].wait_recv()
        if o >= 0:
            vfwd[o] = cm.start(vcell(o, -1), vcell(o, -1), sp=at(0, 1))
        else:
            vfwd[o] = cm.start(vcell(o, 1), vcell(o, 1), sp=at(0, -1))

    def g_round(k):
        gright[k - 1].wait_recv()
        if k < 4:
            gright[k] = cm.start(grow(-k), grow(-k), sp=at(1, 0))
        g_push.append(cm.start(grow(-k), grow(-k), sp=mate))
        if k < 4:
            gleft[k - 1].wait_recv()
            if k < 3:
                gleft[k] = cm.start(grow(k), grow(k), sp=at(-1, 0))
            g_push.append(cm.start(grow(k), grow(k), sp=mate))

    scale_of = 1.0 / D
    wo_push = []

    def wo_arrived():
        l_wo.wait()
        for i, k in enumerate((1, 3, 2)):
            wo_y[i].wait_recv()
            rows = pl.ds(pl.multiple_of(((t + NY - k) % NY) * QC + c * 128, 128), 128)
            wo_push.append(cm.start(wo.at[rows], wo.at[rows], sp=mate))

    def middle(ci):
        for copy in a_y[ci]:
            copy.wait_recv()
        rows = pl.ds(ci * CH, CH)
        nrows = pl.ds(HALO + ci * CH, CH)

        def column(n, total):
            cols = pl.ds(pl.multiple_of(n * 256, 256), 256)
            mid = res[rows, cols].astype(F32) + jnp.dot(att[rows, :], wo[:, cols], preferred_element_type=F32)
            mid = mid.astype(BF16)
            res[rows, cols] = mid
            wide = mid.astype(F32)
            return total + jnp.sum(wide * wide, axis=1, keepdims=True)

        total = lax.fori_loop(0, D // 256, column, jnp.zeros((CH, 1), F32))
        scale = lax.rsqrt(total * scale_of + EPS)

        @pl.loop(0, D // 256)
        def _(n):
            cols = pl.ds(pl.multiple_of(n * 256, 256), 256)
            nrm[nrows, cols] = (res[rows, cols].astype(F32) * scale * gain_ref[:, cols]).astype(BF16)

    def up(tc):
        rows = pl.ds(pl.multiple_of(tc * CH, CH), CH + 2 * HALO)

        @pl.loop(0, FL // 256)
        def _(n):
            cols = pl.ds(pl.multiple_of(n * 256, 256), 256)
            field = nrm[rows, :]

            def convolved(weight, tap):
                u = jnp.dot(field, weight.reshape(D, 256), preferred_element_type=F32)
                u = u.astype(BF16).astype(F32)
                return (
                    u[HALO - 1 : HALO - 1 + CH] * taps_ref[tap : tap + 1, cols]
                    + u[HALO : HALO + CH] * taps_ref[tap + 1 : tap + 2, cols]
                    + u[HALO + 1 : HALO + 1 + CH] * taps_ref[tap + 2 : tap + 3, cols]
                )

            gate = convolved(g[:, :, :, :, cols], 0)
            value = convolved(vd[:, :, :, 0, :, cols], 3)
            hid[:, cols] = (gate / (1.0 + jnp.exp(-gate)) * value).astype(BF16)

    def down(into):
        @pl.loop(0, D // 256)
        def _(n):
            cols = pl.ds(pl.multiple_of(n * 256, 256), 256)
            term = lax.dot_general(hid[...], vd[n, :, :, 1].reshape(256, FL), NT, preferred_element_type=F32)
            into[:, cols] = term.astype(into.dtype)

    attend_chunk(0)
    g_first()
    v_round(1)
    attend_chunk(3)
    send_att(0)
    v_across(0)
    attend_chunk(1)
    send_att(3)
    v_round(2)
    g_round(1)
    attend_chunk(2)
    send_att(1)
    v_across(1)
    v_across(-1)
    l_v.wait()
    v_round(3)
    send_att(2)
    g_round(2)
    v_across(2)
    v_across(-2)
    wo_arrived()
    v_round(4)
    g_round(3)
    v_across(3)
    v_across(-3)
    l_res.wait()
    for copy in wo_push:
        copy.wait_recv()
    middle(0)
    v_across(-4)
    g_round(4)
    middle(3)
    e_high = cm.start(nrm.at[pl.ds(HALO, HALO)], edge.at[1], sp=behind)
    for o in vfwd:
        vfwd[o].wait_recv()
    for k in (1, 2, 3):
        column = vd.at[:, xi(k), c]
        v_cols.append(cm.start(column, column, sp=mate))
    middle(1)
    e_low = cm.start(nrm.at[pl.ds(ROWS, HALO)], edge.at[0], sp=ahead)
    middle(2)
    e_high.wait_recv()
    e_low.wait_recv()
    nrm[0:HALO, :] = jnp.where(s > 0, edge[0].astype(F32), 0.0).astype(BF16)
    nrm[HALO + ROWS :, :] = jnp.where(s < nsp - 1, edge[1].astype(F32), 0.0).astype(BF16)
    for copy in g_push + v_push + v_cols:
        copy.wait_recv()

    up(ty[2])
    down(part.at[0])
    s_right = cm.start(part.at[0, pl.ds(0, 128)], rin.at[0], tp=ty[1])
    s_left = cm.start(part.at[0, pl.ds(128, 128)], rin.at[1], tp=ty[3])
    up(ty[1])
    down(part.at[1])
    b_right = cm.start(part.at[1, pl.ds(128, 128)], fin.at[1], tp=ty[1])
    up(ty[3])
    down(part.at[2])
    a_left = cm.start(part.at[2, pl.ds(0, 128)], fin.at[2], tp=ty[3])
    s_right.wait_recv()

    @pl.loop(0, 8)
    def _(n):
        cols = pl.ds(pl.multiple_of(n * 256, 256), 256)
        part[1, 0:128, cols] = (part[1, 0:128, cols].astype(F32) + rin[0, :, cols].astype(F32)).astype(BF16)

    a_right = cm.start(part.at[1, pl.ds(0, 128)], fin.at[0], tp=ty[1])
    s_left.wait_recv()

    @pl.loop(0, 8)
    def _(n):
        cols = pl.ds(pl.multiple_of(n * 256, 256), 256)
        part[2, 128:256, cols] = (part[2, 128:256, cols].astype(F32) + rin[1, :, cols].astype(F32)).astype(BF16)

    b_left = cm.start(part.at[2, pl.ds(128, 128)], fin.at[3], tp=ty[3])
    up(t)
    down(own)
    for copy in (b_right, a_left, a_right, b_left):
        copy.wait_recv()

    @pl.loop(0, 8)
    def _(n):
        cols = pl.ds(pl.multiple_of(n * 256, 256), 256)
        for i in range(2):
            rows = slice(i * 128, i * 128 + 128)
            mrows = pl.ds(pl.multiple_of(t * CH + i * 128, 128), 128)
            ffn = own[rows, cols] + fin[i, :, cols].astype(F32) + fin[2 + i, :, cols].astype(F32)
            out_ref[rows, cols] = (res[mrows, cols].astype(F32) + ffn).astype(BF16)

    for copy in cm.all:
        copy.wait_send()


def shards(
    residual,
    query,
    key,
    value,
    sink,
    norm_gain,
    w_out,
    w_gate,
    w_value,
    conv_gate,
    conv_value,
    w_down,
):
    offset = lax.axis_index("sp") * ROWS
    positions = (offset - WINDOW + jnp.arange(ROWS + 2 * WINDOW, dtype=jnp.int32)).astype(F32)
    inverse = 1.0 / THETA ** (jnp.arange(0, HD, 2, dtype=F32) / HD)
    angle = positions[:, None] * jnp.tile(inverse, 4)[None, :]
    sign = jnp.where(jnp.arange(128) % HD < HD // 2, -1.0, 1.0).astype(F32)
    cosine = jnp.cos(angle)
    sine = jnp.sin(angle) * sign[None, :]
    kv = jnp.concatenate([key, value], axis=1)
    vd_own = jnp.stack([w_value, w_down.T])
    taps = jnp.concatenate([conv_gate, conv_value], axis=0).astype(F32)
    vmem = pl.BlockSpec(memory_space=pltpu.VMEM)
    hbm = pl.BlockSpec(memory_space=pl.ANY)
    return pl.pallas_call(
        layer,
        out_shape=jax.ShapeDtypeStruct((CH, D), BF16),
        in_specs=[pl.BlockSpec(memory_space=pltpu.SMEM)] + [vmem] * 6 + [hbm] * 4,
        out_specs=vmem,
        scratch_shapes=[
            pltpu.VMEM((ROWS + 2 * WINDOW, 128), BF16),
            pltpu.VMEM((ROWS, QC), BF16),
            pltpu.VMEM((ROWS + 2 * WINDOW, 128), BF16),
            pltpu.VMEM((ROWS + 2 * WINDOW, 128), BF16),
            pltpu.VMEM((ROWS + 2 * WINDOW, 128), BF16),
            pltpu.VMEM((ROWS + 2 * WINDOW, 128), BF16),
            pltpu.VMEM((ROWS, NY * QC), BF16),
            pltpu.VMEM((NY * QC, D), BF16),
            pltpu.VMEM((ROWS, D), BF16),
            pltpu.VMEM((ROWS + 2 * HALO, D), BF16),
            pltpu.VMEM((2, HALO, D), BF16),
            pltpu.VMEM((NZ, NX, NC, 32, FL), BF16),
            pltpu.VMEM((NZ, NX, NC, 2, 32, FL), BF16),
            pltpu.VMEM((CH, FL), BF16),
            pltpu.VMEM((3, CH, D), BF16),
            pltpu.VMEM((CH, D), F32),
            pltpu.VMEM((2, 128, D), BF16),
            pltpu.VMEM((4, 128, D), BF16),
            pltpu.SemaphoreType.DMA((NSEM,)),
            pltpu.SemaphoreType.DMA((NSEM,)),
            pltpu.SemaphoreType.DMA((NLOC,)),
        ],
        compiler_params=pltpu.CompilerParams(
            collective_id=0, has_side_effects=True, vmem_limit_bytes=60 * 1024 * 1024
        ),
        name="layer",
    )(sink, query, kv, cosine, sine, norm_gain.reshape(1, D), taps, residual, w_out, w_gate, vd_own)


def solution(mesh):
    return jax.shard_map(
        shards,
        mesh=mesh,
        in_specs=(
            P("sp", None),
            P("sp", "tp"),
            P("sp", "tp"),
            P("sp", "tp"),
            P("tp"),
            P(),
            P("tp", None),
            P("sp", "tp"),
            P("sp", "tp"),
            P(None, "tp"),
            P(None, "tp"),
            P("tp", "sp"),
        ),
        out_specs=P(("sp", "tp"), None),
        check_vma=False,
    )
```

time: 263 us -> 124 us (0.47)
  the two profiles are of different devices: /device:TPU:7 before, /device:TPU:2 now
where the time goes in v1:
time: 124 us
  Pallas kernels  112 us (90%)
  other arithmetic  7.47 us (6%)
  local copies, waits for them, and re-layouts  4.54 us (4%)
    pallas_call x1, Pallas kernels, shards(): pl.pallas_call(layer, out_shape=jax.ShapeDtypeStruct((CH, D), BF16), in_s...  112 us
    unnamed x3, local copies, waits for them, and re-layouts  4.45 us
    mul x1, other arithmetic, shards(): sine = jnp.sin(angle) * sign[None, :]  3.73 us

profile of v1, /device:TPU:2, one launch (start us, length us, event | category | flops | bytes accessed | tf_op | source)
XLA Modules:
  0.0 124.2 jit_solution(15895666497423445820)
XLA Ops:
  0.0 0.1 mul.31
  0.1 1.3 %maximum_convert_fusion.taps_ref = f32[6,1024]{1,0:T(8,128)} fusion(bf16[3,1024]{1,0:T(4,128)(2,1)} %param.22, bf16[3,1024]{1,0:T(4,128)(2,1)} %param.21), kind=kLoop, calls=%fused_computation.5 | loop fusion | flops 24576 | bytes 36864 | tf_op jit(solution)/shard_map/convert_element_type | solution.py:431
  1.5 1.5 %pad_maximum_fusion.1.vd_hbm = bf16[2,32,1024]{2,1,0:T(8,128)(2,1)} fusion(bf16[1,32,1024]{2,1,0:T(8,128)(2,1)} %bitcast.5, bf16[1,32,1024]{2,1,0:T(8,128)(2,1)} %bitcast.6), kind=kLoop, calls=%fused_computation.4 | loop fusion | flops 65536 | bytes 262144 | tf_op jit(solution)/shard_map/stack | solution.py:430
  3.0 1.1 copy.13
  4.1 1.1 copy.14
  5.2 0.8 pad_maximum_fusion.kv_ref
  6.0 3.7 %fusion = (f32[1280,128]{1,0:T(8,128)}, f32[1280,128]{1,0:T(8,128)}) fusion(f32[128]{0:T(128)S(1)} %compare_select_fusion, f32[128]{0:T(128)S(1)} %mul.31, f32[1280]{0:T(1024)S(1)} %add_convert_fusion), kind=kLoop, calls=%fused_computation.2 | loop fusion | flops 327680 | bytes 1316864 | tf_op jit(solution)/shard_map/mul | solution.py:428
  9.7 112.2 %layer.1 = bf16[256,2048]{1,0:T(8,128)(2,1)} custom-call(f32[4]{0:T(128)} %sink_ref.1, bf16[1024,256]{1,0:T(8,128)(2,1)} %q_ref.1, bf16[1024,128]{1,0:T(8,128)(2,1)} %pad_maximum_fusion.kv_ref, f32[1280,128]{1,0:T(8,128)} %get-tuple-element.6.cos_ref, f32[1280,128]{1,0:T(8,128)} %get-tuple-element.5.sin_ref, f32[1,2048]{1,0:T(1,128)} %bitcast.7, ...), custom_call_target="tpu_custom_call" | custom-call | tf_op jit(solution)/shard_map/layer/pallas_call | solution.py:434
  121.9 2.3 %copy.16 = bf16[256,2048]{1,0:T(8,128)(2,1)} copy(bf16[256,2048]{1,0:T(8,128)(2,1)} %layer.1) | data formatting | bytes 2097152
  (4 shorter events, 0.0 us)

commit v2 on v1

v2 whole, which is shorter than its diff:
```python
import functools

import jax
import jax.numpy as jnp
from jax import lax
from jax.experimental import pallas as pl
from jax.experimental.pallas import tpu as pltpu
from jax.sharding import PartitionSpec as P

HD = 64
WINDOW = 128
THETA = 10000.0
EPS = 1e-06
MESH = pl.DeviceIdType.MESH

NZ, NX, NC, NY = 8, 4, 2, 4
ROWS = 1024
D = 2048
FL = 1024
QC = 256
CH = 256
HALO = 16
NSEM = 184
NLOC = 12
NT = (((1,), (1,)), ((), ()))
F32 = jnp.float32
BF16 = jnp.bfloat16


class Comm:
    def __init__(self, send, recv, local):
        self.send, self.recv, self.local = send, recv, local
        self.count, self.lcount = 0, 0
        self.all = []

    def start(self, src, dst, **where):
        k = self.count
        self.count += 1
        copy = pltpu.make_async_remote_copy(
            src_ref=src,
            dst_ref=dst,
            send_sem=self.send.at[k],
            recv_sem=self.recv.at[k],
            device_id=where,
            device_id_type=MESH,
        )
        copy.start()
        self.all.append(copy)
        return copy

    def here(self, src, dst):
        copy = pltpu.make_async_copy(src, dst, self.local.at[self.lcount])
        self.lcount += 1
        copy.start()
        return copy


def turned(x, cosine, sine):
    lane = lax.broadcasted_iota(jnp.int32, x.shape, 1)
    other = jnp.where((lane & 63) < 32, pltpu.roll(x, 96, 1), pltpu.roll(x, 32, 1))
    return x * cosine + other * sine


def layer(
    sink_ref,
    cos_ref,
    sin_ref,
    q_hbm,
    gain_hbm,
    tap_gate_hbm,
    tap_value_hbm,
    key_hbm,
    value_hbm,
    res_hbm,
    wo_hbm,
    g_hbm,
    v_hbm,
    d_hbm,
    out_ref,
    q_ref,
    gain_ref,
    tap_gate,
    tap_value,
    kvx,
    qr,
    ka,
    kb,
    va,
    vb,
    att,
    wo,
    res,
    nrm,
    edge,
    g,
    v,
    d,
    wdown,
    hid,
    part,
    own,
    rin,
    fin,
    send,
    recv,
    local,
):
    s = lax.axis_index("sp")
    t = lax.axis_index("tp")
    nsp = NZ * NX * NC
    z, x, c = s // (NX * NC), (s // NC) % NX, s % NC

    def at(dz, dx, dc=0):
        return (((z + dz + NZ) % NZ) * NX + (x + dx + NX) % NX) * NC + (c + dc) % NC

    def zi(dz):
        return (z + dz + NZ) % NZ

    def xi(dx):
        return (x + dx + NX) % NX

    ahead, behind = (s + 1) % nsp, (s + nsp - 1) % nsp
    mate = at(0, 0, 1)
    ty = [(t + k) % NY for k in range(NY)]

    cm = Comm(send, recv, local)

    def cell(weight, dz, dx=0):
        return weight.at[zi(dz), xi(dx), c]

    def grow(dz):
        return g.at[zi(dz), :, c]

    l_v, l_d = cm.here(v_hbm, v.at[z, x, c]), cm.here(d_hbm, d.at[z, x, c])
    l_kv = [
        cm.here(key_hbm, kvx.at[0:HD, pl.ds(WINDOW, ROWS)]),
        cm.here(value_hbm, kvx.at[HD : 2 * HD, pl.ds(WINDOW, ROWS)]),
    ]
    l_wo = cm.here(wo_hbm, wo.at[pl.ds(pl.multiple_of(t * QC, QC), QC)])
    l_g = cm.here(g_hbm, g.at[z, x, c])
    l_q = cm.here(q_hbm, q_ref)
    l_small = [cm.here(gain_hbm, gain_ref), cm.here(tap_gate_hbm, tap_gate), cm.here(tap_value_hbm, tap_value)]
    l_res = cm.here(res_hbm, res)

    barrier = pltpu.get_barrier_semaphore()
    peers = [{"sp": i} for i in (ahead, behind, at(1, 0), at(-1, 0), at(0, 1), at(0, 2), at(0, 3), mate)]
    peers += [{"tp": ty[k]} for k in (1, 3)]
    for peer in peers:
        pl.semaphore_signal(barrier, inc=1, device_id=peer, device_id_type=MESH)
    pl.semaphore_wait(barrier, len(peers))

    l_v.wait()

    class Flow:
        def __init__(self, weight):
            self.weight = weight
            self.right, self.left, self.across, self.on = {}, {}, {}, {}
            self.push = []

        def begin(self):
            own = cell(self.weight, 0)
            self.right[0] = cm.start(own, own, sp=at(1, 0))
            self.left[0] = cm.start(own, own, sp=at(-1, 0))

        def share(self, o):
            self.push.append(cm.start(cell(self.weight, o), cell(self.weight, o), sp=mate))

        def spread(self, o):
            one = cell(self.weight, o)
            self.across[o] = (cm.start(one, one, sp=at(0, 1)), cm.start(one, one, sp=at(0, -1)))

        def round(self, k):
            self.right[k - 1].wait_recv()
            if k < 4:
                one = cell(self.weight, -k) if k < 3 else self.weight.at[zi(-k), x, c, pl.ds(0, 16)]
                self.right[k] = cm.start(one, one, sp=at(1, 0))
            self.left[k - 1].wait_recv()
            if k < 4:
                one = cell(self.weight, k) if k < 3 else self.weight.at[zi(k), x, c, pl.ds(16, 16)]
                self.left[k] = cm.start(one, one, sp=at(-1, 0))

        def pass_on(self, o):
            left, right = cell(self.weight, o, -1), cell(self.weight, o, 1)
            self.across[o][0].wait_recv()
            if o >= 0:
                self.on[o] = cm.start(left, left, sp=at(0, 1))
            self.push.append(cm.start(left, left, sp=mate))
            self.across[o][1].wait_recv()
            if o < 0:
                self.on[o] = cm.start(right, right, sp=at(0, -1))
            self.push.append(cm.start(right, right, sp=mate))

        def last(self, o):
            self.on[o].wait_recv()
            self.push.append(cm.start(cell(self.weight, o, 2), cell(self.weight, o, 2), sp=mate))

        def arrived(self):
            for copy in self.push:
                copy.wait_recv()

    fv, fd = Flow(v), Flow(d)
    fv.begin()
    fv.spread(0)
    for copy in l_kv:
        copy.wait()
    h_low = cm.start(kvx.at[:, pl.ds(ROWS, WINDOW)], kvx.at[:, pl.ds(0, WINDOW)], sp=ahead)
    h_high = cm.start(kvx.at[:, pl.ds(WINDOW, WINDOW)], kvx.at[:, pl.ds(WINDOW + ROWS, WINDOW)], sp=behind)
    l_wo.wait()

    def worows(k, at_row=0, count=128):
        return wo.at[pl.ds(pl.multiple_of(((t + k) % NY) * QC + c * 128 + at_row, 64), count)]

    wo_right = cm.start(worows(0), worows(0), tp=ty[1])
    wo_left = cm.start(worows(0), worows(0), tp=ty[3])
    l_g.wait()
    g_x = [cm.start(g.at[z, x, c], g.at[z, x, c], sp=at(0, k)) for k in (1, 3, 2)]
    fv.share(0)
    l_d.wait()
    fd.spread(0)

    def table(b):
        base = pl.ds(WINDOW + b, 1)
        cb, sb = cos_ref[base, :], sin_ref[base, :]
        cr, sr = cos_ref[0:WINDOW, :], sin_ref[0:WINDOW, :]
        lane = lax.broadcasted_iota(jnp.int32, (WINDOW, 128), 1)
        sine = sb * cr + cb * sr
        return cb * cr - sb * sr, jnp.where((lane & 63) < 32, -sine, sine)

    def prepare(b, with_query):
        cosine, sine = table(b)
        rows = pl.ds(pl.multiple_of(b * WINDOW, WINDOW), WINDOW)
        if with_query:
            qrows = pl.ds(pl.multiple_of(b * WINDOW - WINDOW, WINDOW), WINDOW)
            for p in range(2):
                lanes = slice(p * 128, p * 128 + 128)
                qr[qrows, lanes] = turned(q_ref[qrows, lanes].astype(F32), cosine, sine).astype(BF16)
        both = kvx[:, rows].astype(F32).T
        lane = lax.broadcasted_iota(jnp.int32, both.shape, 1)
        keys = jnp.where(lane < HD, turned(both, cosine, sine), 0.0)
        values = jnp.where(lane < HD, 0.0, both)
        ka[rows, :] = keys.astype(BF16)
        kb[rows, :] = pltpu.roll(keys, HD, 1).astype(BF16)
        va[rows, :] = pltpu.roll(values, HD, 1).astype(BF16)
        vb[rows, :] = values.astype(BF16)

    l_q.wait()

    @pl.loop(1, ROWS // WINDOW + 1)
    def _(b):
        prepare(b, True)

    h_low.wait_recv()
    h_high.wait_recv()

    @pl.loop(0, 2)
    def _(i):
        prepare(i * (ROWS // WINDOW + 1), False)

    def attend(b):
        start = pl.multiple_of(b * WINDOW, WINDOW)
        rows = pl.ds(start, WINDOW)
        band = pl.ds(start, 3 * WINDOW)
        r = lax.broadcasted_iota(jnp.int32, (WINDOW, 3 * WINDOW), 0)
        j = lax.broadcasted_iota(jnp.int32, (WINDOW, 3 * WINDOW), 1)
        first = s * ROWS + start - WINDOW
        valid = (j >= r) & (j <= r + 2 * WINDOW) & (j + first >= 0) & (j + first < nsp * ROWS)
        lane = lax.broadcasted_iota(jnp.int32, (WINDOW, 128), 1)
        vv = jnp.concatenate([va[band, :], vb[band, :]], axis=0)
        for p in range(2):
            qp = qr[rows, p * 128 : p * 128 + 128]
            weights, inverse = [], []
            for i, keys in enumerate((ka, kb)):
                sc = lax.dot_general(qp, keys[band, :], NT, preferred_element_type=F32)
                sc = jnp.where(valid, sc * HD ** (-0.5), -1e30)
                sink = sink_ref[2 * p + i]
                top = jnp.maximum(jnp.max(sc, axis=1, keepdims=True), sink)
                w = jnp.exp(sc - top)
                denom = jnp.sum(w, axis=1, keepdims=True) + jnp.exp(sink - top)
                weights.append(w.astype(BF16))
                inverse.append(1.0 / denom)
            o = jnp.dot(jnp.concatenate(weights, axis=1), vv, preferred_element_type=F32)
            o = o * jnp.where(lane < HD, inverse[0], inverse[1])
            att[rows, pl.ds(pl.multiple_of(t * QC + p * 128, 128), 128)] = o.astype(BF16)

    def attend_chunk(ci):
        @pl.loop(0, 2)
        def _(i):
            attend(ci * 2 + i)

    a_y, a_on = {}, {}

    def send_att(ci):
        piece = att.at[pl.ds(ci * CH, CH), pl.ds(pl.multiple_of(t * QC, QC), QC)]
        a_y[ci] = (cm.start(piece, piece, tp=ty[1]), cm.start(piece, piece, tp=ty[3]))

    def pass_att(ci):
        a_y[ci][0].wait_recv()
        piece = att.at[pl.ds(ci * CH, 128), pl.ds(pl.multiple_of(ty[3] * QC, QC), QC)]
        right = cm.start(piece, piece, tp=ty[1])
        a_y[ci][1].wait_recv()
        piece = att.at[pl.ds(ci * CH + 128, 128), pl.ds(pl.multiple_of(ty[1] * QC, QC), QC)]
        a_on[ci] = (right, cm.start(piece, piece, tp=ty[3]))

    wo_on, wo_push = [], []

    def pass_wo():
        wo_right.wait_recv()
        wo_on.append(cm.start(worows(3, 0, 64), worows(3, 0, 64), tp=ty[1]))
        wo_push.append(cm.start(worows(3), worows(3), sp=mate))
        wo_left.wait_recv()
        wo_on.append(cm.start(worows(1, 64, 64), worows(1, 64, 64), tp=ty[3]))
        wo_push.append(cm.start(worows(1), worows(1), sp=mate))

    def last_wo():
        for copy in wo_on:
            copy.wait_recv()
        wo_push.append(cm.start(worows(2), worows(2), sp=mate))

    gright, gleft, g_push = {}, {}, []

    def g_first():
        for copy in g_x:
            copy.wait_recv()
        gright[0] = cm.start(grow(0), grow(0), sp=at(1, 0))
        gleft[0] = cm.start(grow(0), grow(0), sp=at(-1, 0))
        g_push.append(cm.start(grow(0), grow(0), sp=mate))

    def g_round(k):
        gright[k - 1].wait_recv()
        if k < 4:
            block = grow(-k) if k < 3 else g.at[zi(-k), pl.ds(0, 2), c]
            gright[k] = cm.start(block, block, sp=at(1, 0))
        gleft[k - 1].wait_recv()
        if k < 4:
            block = grow(k) if k < 3 else g.at[zi(k), pl.ds(2, 2), c]
            gleft[k] = cm.start(block, block, sp=at(-1, 0))
            g_push.append(cm.start(grow(k), grow(k), sp=mate))
        g_push.append(cm.start(grow(-k), grow(-k), sp=mate))

    def middle(ci):
        for copy in a_on[ci]:
            copy.wait_recv()
        rows = pl.ds(ci * CH, CH)
        nrows = pl.ds(HALO + ci * CH, CH)
        total = jnp.zeros((CH, 1), F32)
        for n in range(D // 512):
            cols = slice(n * 512, n * 512 + 512)
            mid = res[rows, cols].astype(F32) + jnp.dot(att[rows, :], wo[:, cols], preferred_element_type=F32)
            mid = mid.astype(BF16)
            res[rows, cols] = mid
            wide = mid.astype(F32)
            total = total + jnp.sum(wide * wide, axis=1, keepdims=True)
        scale = lax.rsqrt(total / D + EPS)
        for n in range(D // 512):
            cols = slice(n * 512, n * 512 + 512)
            nrm[nrows, cols] = (res[rows, cols].astype(F32) * scale * gain_ref[:, cols]).astype(BF16)

    def up(tc):
        rows = pl.ds(pl.multiple_of(tc * CH, CH), CH + 2 * HALO)
        for n in range(FL // 512):
            cols = slice(n * 512, n * 512 + 512)

            def convolved(weight, taps_ref):
                u = jnp.dot(nrm[rows, :], weight.reshape(D, 512), preferred_element_type=F32)
                u = u.astype(BF16).astype(F32)
                taps = taps_ref[:, cols].astype(F32)
                return (
                    u[HALO - 1 : HALO - 1 + CH] * taps[0:1]
                    + u[HALO : HALO + CH] * taps[1:2]
                    + u[HALO + 1 : HALO + 1 + CH] * taps[2:3]
                )

            gate = convolved(g[:, :, :, :, cols], tap_gate)
            value = convolved(v[:, :, :, :, cols], tap_value)
            hid[:, cols] = (gate / (1.0 + jnp.exp(-gate)) * value).astype(BF16)

    def turn_down():
        for n in range(NZ):
            wdown[:, n * 256 : n * 256 + 256] = d[n].reshape(256, FL).T

    def down(into, tiles=range(D // 512)):
        for n in tiles:
            cols = slice(n * 512, n * 512 + 512)
            into[:, cols] = jnp.dot(hid[...], wdown[:, cols], preferred_element_type=F32).astype(into.dtype)

    attend_chunk(0)
    fv.round(1)
    for o in (1, -1):
        fv.spread(o)
        fv.share(o)
    fv.pass_on(0)
    fd.begin()
    attend_chunk(3)
    send_att(0)
    fv.round(2)
    g_first()
    for o in (2, -2):
        fv.spread(o)
        fv.share(o)
    attend_chunk(1)
    send_att(3)
    fd.round(1)
    fd.spread(1)
    fd.spread(-1)
    attend_chunk(2)
    fv.pass_on(1)
    fv.pass_on(-1)
    fd.pass_on(0)
    fv.last(0)
    fv.round(3)
    for o in (3, -3):
        fv.spread(o)
        fv.share(o)
    pass_wo()
    send_att(1)
    send_att(2)
    fd.round(2)
    g_round(1)
    fv.round(4)
    fv.spread(-4)
    fv.share(-4)
    fd.spread(2)
    fd.spread(-2)
    fv.pass_on(2)
    fv.pass_on(-2)
    fv.last(1)
    fv.last(-1)
    fd.share(0)
    pass_att(0)
    pass_att(3)
    fd.pass_on(1)
    fd.pass_on(-1)
    fd.round(3)
    fd.spread(3)
    fd.spread(-3)
    last_wo()
    fv.pass_on(3)
    fv.pass_on(-3)
    fv.pass_on(-4)
    pass_att(1)
    g_round(2)
    fd.round(4)
    fd.spread(-4)
    pass_att(2)
    for copy in [l_res] + l_small:
        copy.wait()
    fv.last(2)
    fv.last(-2)
    for o in (1, -1, 2, -2):
        fd.share(o)
    for copy in wo_push:
        copy.wait_recv()
    middle(0)
    fd.pass_on(2)
    fd.pass_on(-2)
    middle(3)
    g_round(3)
    e_high = cm.start(nrm.at[pl.ds(HALO, HALO)], edge.at[1], sp=behind)
    fd.pass_on(3)
    fd.pass_on(-3)
    fd.pass_on(-4)
    middle(1)
    e_low = cm.start(nrm.at[pl.ds(ROWS, HALO)], edge.at[0], sp=ahead)
    for o in (3, -3, -4):
        fv.last(o)
    for o in (0, 1, -1, 2, -2):
        fd.last(o)
    middle(2)
    g_round(4)
    for o in (3, -3, -4):
        fd.share(o)
        fd.last(o)
    fv.arrived()
    for copy in g_push:
        copy.wait_recv()
    e_high.wait_recv()
    e_low.wait_recv()
    nrm[0:HALO, :] = jnp.where(s > 0, edge[0].astype(F32), 0.0).astype(BF16)
    nrm[HALO + ROWS :, :] = jnp.where(s < nsp - 1, edge[1].astype(F32), 0.0).astype(BF16)
    fd.arrived()
    turn_down()
    up(ty[2])
    sides = (slice(0, D // 2), slice(D // 2, D))
    s_right, s_left = [], []
    for i, side in enumerate(sides):
        down(part.at[0], (2 * i, 2 * i + 1))
        s_right.append(cm.start(part.at[0, 0:128, side], rin.at[0, :, side], tp=ty[1]))
        s_left.append(cm.start(part.at[0, 128:256, side], rin.at[1, :, side], tp=ty[3]))
    up(ty[1])
    down(part.at[1])
    b_right = cm.start(part.at[1, 128:256], fin.at[1], tp=ty[1])
    up(ty[3])
    down(part.at[2])
    a_left = cm.start(part.at[2, 0:128], fin.at[2], tp=ty[3])

    def joined(which, rows, side):
        base = 0 if side.start == 0 else D // 2

        @pl.loop(0, 4)
        def _(n):
            cols = pl.ds(pl.multiple_of(base + n * 256, 256), 256)
            total = part[1 + which, rows, cols].astype(F32) + rin[which, :, cols].astype(F32)
            part[1 + which, rows, cols] = total.astype(BF16)

    a_right, b_left = [], []
    for i, side in enumerate(sides):
        s_right[i].wait_recv()
        joined(0, slice(0, 128), side)
        a_right.append(cm.start(part.at[1, 0:128, side], fin.at[0, :, side], tp=ty[1]))
        s_left[i].wait_recv()
        joined(1, slice(128, 256), side)
        b_left.append(cm.start(part.at[2, 128:256, side], fin.at[3, :, side], tp=ty[3]))
    up(t)
    down(own)
    b_right.wait_recv()
    a_left.wait_recv()
    for i, side in enumerate(sides):
        a_right[i].wait_recv()
        b_left[i].wait_recv()

        @pl.loop(4 * i, 4 * i + 4)
        def _(n):
            cols = pl.ds(pl.multiple_of(n * 256, 256), 256)
            for k in range(2):
                rows = slice(k * 128, k * 128 + 128)
                mrows = pl.ds(pl.multiple_of(t * CH + k * 128, 128), 128)
                ffn = own[rows, cols] + fin[k, :, cols].astype(F32) + fin[2 + k, :, cols].astype(F32)
                out_ref[rows, cols] = (res[mrows, cols].astype(F32) + ffn).astype(BF16)

    for copy in cm.all:
        copy.wait_send()


def shards(
    residual,
    query,
    key,
    value,
    sink,
    norm_gain,
    w_out,
    w_gate,
    w_value,
    conv_gate,
    conv_value,
    w_down,
):
    offset = lax.axis_index("sp") * ROWS
    inverse = 1.0 / THETA ** (jnp.arange(0, HD, 2, dtype=F32) / HD)
    within = jnp.arange(WINDOW, dtype=jnp.int32)
    starts = offset + (jnp.arange(16, dtype=jnp.int32) - 1) * WINDOW
    positions = jnp.concatenate([within, starts]).astype(F32)
    angle = positions[:, None] * jnp.tile(inverse, 4)[None, :]
    vmem = pl.BlockSpec(memory_space=pltpu.VMEM)
    hbm = pl.BlockSpec(memory_space=pl.ANY)
    return pl.pallas_call(
        layer,
        out_shape=jax.ShapeDtypeStruct((CH, D), BF16),
        in_specs=[pl.BlockSpec(memory_space=pltpu.SMEM)] + [vmem] * 2 + [hbm] * 11,
        out_specs=vmem,
        scratch_shapes=[
            pltpu.VMEM((ROWS, QC), BF16),
            pltpu.VMEM((1, D), F32),
            pltpu.VMEM((3, FL), BF16),
            pltpu.VMEM((3, FL), BF16),
            pltpu.VMEM((2 * HD, ROWS + 2 * WINDOW), BF16),
            pltpu.VMEM((ROWS, QC), BF16),
            pltpu.VMEM((ROWS + 2 * WINDOW, 128), BF16),
            pltpu.VMEM((ROWS + 2 * WINDOW, 128), BF16),
            pltpu.VMEM((ROWS + 2 * WINDOW, 128), BF16),
            pltpu.VMEM((ROWS + 2 * WINDOW, 128), BF16),
            pltpu.VMEM((ROWS, NY * QC), BF16),
            pltpu.VMEM((NY * QC, D), BF16),
            pltpu.VMEM((ROWS, D), BF16),
            pltpu.VMEM((ROWS + 2 * HALO, D), BF16),
            pltpu.VMEM((2, HALO, D), BF16),
            pltpu.VMEM((NZ, NX, NC, 32, FL), BF16),
            pltpu.VMEM((NZ, NX, NC, 32, FL), BF16),
            pltpu.VMEM((NZ, NX, NC, 32, FL), BF16),
            pltpu.VMEM((FL, D), BF16),
            pltpu.VMEM((CH, FL), BF16),
            pltpu.VMEM((3, CH, D), BF16),
            pltpu.VMEM((CH, D), F32),
            pltpu.VMEM((2, 128, D), BF16),
            pltpu.VMEM((4, 128, D), BF16),
            pltpu.SemaphoreType.DMA((NSEM,)),
            pltpu.SemaphoreType.DMA((NSEM,)),
            pltpu.SemaphoreType.DMA((NLOC,)),
        ],
        compiler_params=pltpu.CompilerParams(
            collective_id=0, has_side_effects=True, vmem_limit_bytes=62 * 1024 * 1024
        ),
        name="layer",
    )(
        sink,
        jnp.cos(angle),
        jnp.sin(angle),
        query,
        norm_gain.reshape(1, D),
        conv_gate,
        conv_value,
        key.T,
        value.T,
        residual,
        w_out,
        w_gate,
        w_value,
        w_down.T,
    )


def solution(mesh):
    return jax.shard_map(
        shards,
        mesh=mesh,
        in_specs=(
            P("sp", None),
            P("sp", "tp"),
            P("sp", "tp"),
            P("sp", "tp"),
            P("tp"),
            P(),
            P("tp", None),
            P("sp", "tp"),
            P("sp", "tp"),
            P(None, "tp"),
            P(None, "tp"),
            P("tp", "sp"),
        ),
        out_specs=P(("sp", "tp"), None),
        check_vma=False,
    )
```

time: 124 us -> 103 us (0.83)
  the two profiles are of different devices: /device:TPU:2 before, /device:TPU:1 now
where the time goes in v2:
time: 103 us; the launch traced here: 102 us
  Pallas kernels  99 us (96%)
  local copies, waits for them, and re-layouts  2.39 us (2%)
  other arithmetic  1.03 us (1%)
    pallas_call x1, Pallas kernels, shards(): pl.pallas_call(layer, out_shape=jax.ShapeDtypeStruct((CH, D), BF16), in_s...  99 us
    unnamed x1, local copies, waits for them, and re-layouts  2.3 us

profile of v2, /device:TPU:1, one launch (start us, length us, event | category | flops | bytes accessed | tf_op | source)
XLA Modules:
  0.0 102.5 jit_solution(14402561101132343467)
XLA Ops:
  0.1 0.1 mul.29
  0.1 1.0 multiply_sine_fusion
  1.1 99.0 %layer.1 = bf16[256,2048]{1,0:T(8,128)(2,1)} custom-call(f32[4]{0:T(128)} %sink_ref.1, f32[144,128]{1,0:T(8,128)} %get-tuple-element.6.cos_ref, f32[144,128]{1,0:T(8,128)} %get-tuple-element.5.sin_ref, bf16[1024,256]{1,0:T(8,128)(2,1)} %q_hbm.1, f32[1,2048]{1,0:T(1,128)} %bitcast.7, bf16[3,1024]{1,0:T(4,128)(2,1)} %tap_gate_hbm.1, ...), custom_call_target="tpu_custom_call" | custom-call | tf_op jit(solution)/shard_map/layer/pallas_call | solution.py:556
  100.2 2.3 %copy.14 = bf16[256,2048]{1,0:T(8,128)(2,1)} copy(bf16[256,2048]{1,0:T(8,128)(2,1)} %layer.1) | data formatting | bytes 2097152
  (5 shorter events, 0.0 us)

commit v3 on v2

--- a/solution.py
+++ b/solution.py
@@ -20,33 +20,61 @@
 QC = 256
 CH = 256
 HALO = 16
-NSEM = 184
+NSEND = 6
+NRECV = 64
 NLOC = 12
 NT = (((1,), (1,)), ((), ()))
 F32 = jnp.float32
 BF16 = jnp.bfloat16
 
 
+class Slot:
+    def __init__(self, comm, index):
+        self.comm, self.sem = comm, comm.recv.at[index]
+        self.size, self.done = 0, False
+
+    def wait_recv(self):
+        if not self.done:
+            self.done = True
+            self.comm.wait(self.sem, self.size)
+
+
 class Comm:
-    def __init__(self, send, recv, local):
-        self.send, self.recv, self.local = send, recv, local
-        self.count, self.lcount = 0, 0
-        self.all = []
-
-    def start(self, src, dst, **where):
-        k = self.count
-        self.count += 1
+    def __init__(self, send, recv, local, filler):
+        self.send, self.recv, self.local, self.filler = send, recv, local, filler
+        self.slots, self.lcount = 0, 0
+        self.groups = {}
+
+    def slot(self):
+        assert self.slots < NRECV
+        self.slots += 1
+        return Slot(self, self.slots - 1)
+
+    def wait(self, sem, size):
+        view = self.filler.at[0 : size // (2 * D)]
+        pltpu.make_async_copy(view, view, sem).wait()
+
+    def start(self, src, dst, slot=None, group="rest", **where):
+        slot = slot or self.slot()
+        assert not slot.done
+        if group not in self.groups:
+            assert len(self.groups) < NSEND
+            self.groups[group] = [self.send.at[len(self.groups)], 0]
+        size = 2
+        for extent in src.shape:
+            size *= extent
+        slot.size += size
+        self.groups[group][1] += size
         copy = pltpu.make_async_remote_copy(
             src_ref=src,
             dst_ref=dst,
-            send_sem=self.send.at[k],
-            recv_sem=self.recv.at[k],
+            send_sem=self.groups[group][0],
+            recv_sem=slot.sem,
             device_id=where,
             device_id_type=MESH,
         )
         copy.start()
-        self.all.append(copy)
-        return copy
+        return slot
 
     def here(self, src, dst):
         copy = pltpu.make_async_copy(src, dst, self.local.at[self.lcount])
@@ -54,6 +82,10 @@
         copy.start()
         return copy
 
+    def sent(self):
+        for sem, size in self.groups.values():
+            self.wait(sem, size)
+
 
 def turned(x, cosine, sine):
     lane = lax.broadcasted_iota(jnp.int32, x.shape, 1)
@@ -63,8 +95,7 @@
 
 def layer(
     sink_ref,
-    cos_ref,
-    sin_ref,
+    inverse_ref,
     q_hbm,
     gain_hbm,
     tap_gate_hbm,
@@ -77,6 +108,8 @@
     v_hbm,
     d_hbm,
     out_ref,
+    cos_ref,
+    sin_ref,
     q_ref,
     gain_ref,
     tap_gate,
@@ -123,7 +156,7 @@
     mate = at(0, 0, 1)
     ty = [(t + k) % NY for k in range(NY)]
 
-    cm = Comm(send, recv, local)
+    cm = Comm(send, recv, local, nrm)
 
     def cell(weight, dz, dx=0):
         return weight.at[zi(dz), xi(dx), c]
@@ -147,73 +180,86 @@
     peers += [{"tp": ty[k]} for k in (1, 3)]
     for peer in peers:
         pl.semaphore_signal(barrier, inc=1, device_id=peer, device_id_type=MESH)
+    row = lax.broadcasted_iota(jnp.int32, (WINDOW + 16, 128), 0)
+    place = jnp.where(row < WINDOW, row, s * ROWS + (row - WINDOW - 1) * WINDOW).astype(F32)
+    angle = place * inverse_ref[...]
+    cos_ref[...] = jnp.cos(angle)
+    sin_ref[...] = jnp.sin(angle)
     pl.semaphore_wait(barrier, len(peers))
 
     l_v.wait()
 
     class Flow:
-        def __init__(self, weight):
-            self.weight = weight
-            self.right, self.left, self.across, self.on = {}, {}, {}, {}
-            self.push = []
+        def __init__(self, weight, group):
+            self.weight, self.group = weight, group
+            self.ring, self.across, self.on = {}, {}, {}
+            self.push = cm.slot()
+
+        def start(self, ref, slot, **where):
+            return cm.start(ref, ref, slot, self.group, **where)
 
         def begin(self):
-            own = cell(self.weight, 0)
-            self.right[0] = cm.start(own, own, sp=at(1, 0))
-            self.left[0] = cm.start(own, own, sp=at(-1, 0))
-
-        def share(self, o):
-            self.push.append(cm.start(cell(self.weight, o), cell(self.weight, o), sp=mate))
+            own, self.ring[0] = cell(self.weight, 0), cm.slot()
+            self.start(own, self.ring[0], sp=at(1, 0))
+            self.start(own, self.ring[0], sp=at(-1, 0))
+
+        def share(self, o, dx=0):
+            self.start(cell(self.weight, o, dx), self.push, sp=mate)
 
         def spread(self, o):
-            one = cell(self.weight, o)
-            self.across[o] = (cm.start(one, one, sp=at(0, 1)), cm.start(one, one, sp=at(0, -1)))
+            one, self.across[o] = cell(self.weight, o), cm.slot()
+            self.start(one, self.across[o], sp=at(0, 1))
+            self.start(one, self.across[o], sp=at(0, -1))
 
         def round(self, k):
-            self.right[k - 1].wait_recv()
+            self.ring[k - 1].wait_recv()
             if k < 4:
-                one = cell(self.weight, -k) if k < 3 else self.weight.at[zi(-k), x, c, pl.ds(0, 16)]
-                self.right[k] = cm.start(one, one, sp=at(1, 0))
-            self.left[k - 1].wait_recv()
-            if k < 4:
-                one = cell(self.weight, k) if k < 3 else self.weight.at[zi(k), x, c, pl.ds(16, 16)]
-                self.left[k] = cm.start(one, one, sp=at(-1, 0))
+                low, high = cell(self.weight, -k), cell(self.weight, k)
+                if k == 3:
+                    low = self.weight.at[zi(-k), x, c, pl.ds(0, 16)]
+                    high = self.weight.at[zi(k), x, c, pl.ds(16, 16)]
+                self.ring[k] = cm.slot()
+                self.start(low, self.ring[k], sp=at(1, 0))
+                self.start(high, self.ring[k], sp=at(-1, 0))
 
         def pass_on(self, o):
-            left, right = cell(self.weight, o, -1), cell(self.weight, o, 1)
-            self.across[o][0].wait_recv()
+            self.across[o].wait_recv()
+            if abs(o) not in self.on:
+                self.on[abs(o)] = cm.slot()
             if o >= 0:
-                self.on[o] = cm.start(left, left, sp=at(0, 1))
-            self.push.append(cm.start(left, left, sp=mate))
-            self.across[o][1].wait_recv()
-            if o < 0:
-                self.on[o] = cm.start(right, right, sp=at(0, -1))
-            self.push.append(cm.start(right, right, sp=mate))
+                self.start(cell(self.weight, o, -1), self.on[abs(o)], sp=at(0, 1))
+            else:
+                self.start(cell(self.weight, o, 1), self.on[abs(o)], sp=at(0, -1))
+            self.share(o, -1)
+            self.share(o, 1)
 
         def last(self, o):
-            self.on[o].wait_recv()
-            self.push.append(cm.start(cell(self.weight, o, 2), cell(self.weight, o, 2), sp=mate))
+            self.on[abs(o)].wait_recv()
+            self.share(o, 2)
 
         def arrived(self):
-            for copy in self.push:
-                copy.wait_recv()
-
-    fv, fd = Flow(v), Flow(d)
+            self.push.wait_recv()
+
+    fv, fd = Flow(v, "v"), Flow(d, "d")
     fv.begin()
     fv.spread(0)
     for copy in l_kv:
         copy.wait()
-    h_low = cm.start(kvx.at[:, pl.ds(ROWS, WINDOW)], kvx.at[:, pl.ds(0, WINDOW)], sp=ahead)
-    h_high = cm.start(kvx.at[:, pl.ds(WINDOW, WINDOW)], kvx.at[:, pl.ds(WINDOW + ROWS, WINDOW)], sp=behind)
+    halo = cm.slot()
+    h_low = cm.start(kvx.at[:, pl.ds(ROWS, WINDOW)], kvx.at[:, pl.ds(0, WINDOW)], halo, sp=ahead)
+    h_high = cm.start(kvx.at[:, pl.ds(WINDOW, WINDOW)], kvx.at[:, pl.ds(WINDOW + ROWS, WINDOW)], halo, sp=behind)
     l_wo.wait()
 
     def worows(k, at_row=0, count=128):
         return wo.at[pl.ds(pl.multiple_of(((t + k) % NY) * QC + c * 128 + at_row, 64), count)]
 
-    wo_right = cm.start(worows(0), worows(0), tp=ty[1])
-    wo_left = cm.start(worows(0), worows(0), tp=ty[3])
+    wo_first, wo_on, wo_push = cm.slot(), cm.slot(), cm.slot()
+    cm.start(worows(0), worows(0), wo_first, "wo", tp=ty[1])
+    cm.start(worows(0), worows(0), wo_first, "wo", tp=ty[3])
     l_g.wait()
-    g_x = [cm.start(g.at[z, x, c], g.at[z, x, c], sp=at(0, k)) for k in (1, 3, 2)]
+    g_x, g_push = cm.slot(), cm.slot()
+    for k in (1, 3, 2):
+        cm.start(g.at[z, x, c], g.at[z, x, c], g_x, "g", sp=at(0, k))
     fv.share(0)
     l_d.wait()
     fd.spread(0)
@@ -291,55 +337,55 @@
 
     def send_att(ci):
         piece = att.at[pl.ds(ci * CH, CH), pl.ds(pl.multiple_of(t * QC, QC), QC)]
-        a_y[ci] = (cm.start(piece, piece, tp=ty[1]), cm.start(piece, piece, tp=ty[3]))
+        a_y[ci] = cm.slot()
+        cm.start(piece, piece, a_y[ci], tp=ty[1])
+        cm.start(piece, piece, a_y[ci], tp=ty[3])
 
     def pass_att(ci):
-        a_y[ci][0].wait_recv()
+        a_y[ci].wait_recv()
+        a_on[ci] = cm.slot()
         piece = att.at[pl.ds(ci * CH, 128), pl.ds(pl.multiple_of(ty[3] * QC, QC), QC)]
-        right = cm.start(piece, piece, tp=ty[1])
-        a_y[ci][1].wait_recv()
+        cm.start(piece, piece, a_on[ci], tp=ty[1])
         piece = att.at[pl.ds(ci * CH + 128, 128), pl.ds(pl.multiple_of(ty[1] * QC, QC), QC)]
-        a_on[ci] = (right, cm.start(piece, piece, tp=ty[3]))
-
-    wo_on, wo_push = [], []
+        cm.start(piece, piece, a_on[ci], tp=ty[3])
 
     def pass_wo():
-        wo_right.wait_recv()
-        wo_on.append(cm.start(worows(3, 0, 64), worows(3, 0, 64), tp=ty[1]))
-        wo_push.append(cm.start(worows(3), worows(3), sp=mate))
-        wo_left.wait_recv()
-        wo_on.append(cm.start(worows(1, 64, 64), worows(1, 64, 64), tp=ty[3]))
-        wo_push.append(cm.start(worows(1), worows(1), sp=mate))
+        wo_first.wait_recv()
+        cm.start(worows(3, 0, 64), worows(3, 0, 64), wo_on, "wo", tp=ty[1])
+        cm.start(worows(1, 64, 64), worows(1, 64, 64), wo_on, "wo", tp=ty[3])
+        cm.start(worows(3), worows(3), wo_push, "wo", sp=mate)
+        cm.start(worows(1), worows(1), wo_push, "wo", sp=mate)
 
     def last_wo():
-        for copy in wo_on:
-            copy.wait_recv()
-        wo_push.append(cm.start(worows(2), worows(2), sp=mate))
-
-    gright, gleft, g_push = {}, {}, []
+        wo_on.wait_recv()
+        cm.start(worows(2), worows(2), wo_push, "wo", sp=mate)
+
+    g_ring = {}
+
+    def g_send(ref, slot, where):
+        cm.start(ref, ref, slot, "g", sp=where)
 
     def g_first():
-        for copy in g_x:
-            copy.wait_recv()
-        gright[0] = cm.start(grow(0), grow(0), sp=at(1, 0))
-        gleft[0] = cm.start(grow(0), grow(0), sp=at(-1, 0))
-        g_push.append(cm.start(grow(0), grow(0), sp=mate))
+        g_x.wait_recv()
+        g_ring[0] = cm.slot()
+        g_send(grow(0), g_ring[0], at(1, 0))
+        g_send(grow(0), g_ring[0], at(-1, 0))
+        g_send(grow(0), g_push, mate)
 
     def g_round(k):
-        gright[k - 1].wait_recv()
+        g_ring[k - 1].wait_recv()
         if k < 4:
-            block = grow(-k) if k < 3 else g.at[zi(-k), pl.ds(0, 2), c]
-            gright[k] = cm.start(block, block, sp=at(1, 0))
-        gleft[k - 1].wait_recv()
-        if k < 4:
-            block = grow(k) if k < 3 else g.at[zi(k), pl.ds(2, 2), c]
-            gleft[k] = cm.start(block, block, sp=at(-1, 0))
-            g_push.append(cm.start(grow(k), grow(k), sp=mate))
-        g_push.append(cm.start(grow(-k), grow(-k), sp=mate))
+            low, high = grow(-k), grow(k)
+            if k == 3:
+                low, high = g.at[zi(-k), pl.ds(0, 2), c], g.at[zi(k), pl.ds(2, 2), c]
+            g_ring[k] = cm.slot()
+            g_send(low, g_ring[k], at(1, 0))
+            g_send(high, g_ring[k], at(-1, 0))
+            g_send(grow(k), g_push, mate)
+        g_send(grow(-k), g_push, mate)
 
     def middle(ci):
-        for copy in a_on[ci]:
-            copy.wait_recv()
+        a_on[ci].wait_recv()
         rows = pl.ds(ci * CH, CH)
         nrows = pl.ds(HALO + ci * CH, CH)
         total = jnp.zeros((CH, 1), F32)
@@ -448,19 +494,19 @@
     fv.last(-2)
     for o in (1, -1, 2, -2):
         fd.share(o)
-    for copy in wo_push:
-        copy.wait_recv()
+    wo_push.wait_recv()
     middle(0)
     fd.pass_on(2)
     fd.pass_on(-2)
     middle(3)
     g_round(3)
-    e_high = cm.start(nrm.at[pl.ds(HALO, HALO)], edge.at[1], sp=behind)
+    e_both = cm.slot()
+    cm.start(nrm.at[pl.ds(HALO, HALO)], edge.at[1], e_both, sp=behind)
     fd.pass_on(3)
     fd.pass_on(-3)
     fd.pass_on(-4)
     middle(1)
-    e_low = cm.start(nrm.at[pl.ds(ROWS, HALO)], edge.at[0], sp=ahead)
+    cm.start(nrm.at[pl.ds(ROWS, HALO)], edge.at[0], e_both, sp=ahead)
     for o in (3, -3, -4):
         fv.last(o)
     for o in (0, 1, -1, 2, -2):
@@ -471,27 +517,27 @@
         fd.share(o)
         fd.last(o)
     fv.arrived()
-    for copy in g_push:
-        copy.wait_recv()
-    e_high.wait_recv()
-    e_low.wait_recv()
+    g_push.wait_recv()
+    e_both.wait_recv()
     nrm[0:HALO, :] = jnp.where(s > 0, edge[0].astype(F32), 0.0).astype(BF16)
     nrm[HALO + ROWS :, :] = jnp.where(s < nsp - 1, edge[1].astype(F32), 0.0).astype(BF16)
     fd.arrived()
     turn_down()
     up(ty[2])
     sides = (slice(0, D // 2), slice(D // 2, D))
-    s_right, s_left = [], []
+    s_both = []
     for i, side in enumerate(sides):
         down(part.at[0], (2 * i, 2 * i + 1))
-        s_right.append(cm.start(part.at[0, 0:128, side], rin.at[0, :, side], tp=ty[1]))
-        s_left.append(cm.start(part.at[0, 128:256, side], rin.at[1, :, side], tp=ty[3]))
+        s_both.append(cm.slot())
+        cm.start(part.at[0, 0:128, side], rin.at[0, :, side], s_both[i], "sum", tp=ty[1])
+        cm.start(part.at[0, 128:256, side], rin.at[1, :, side], s_both[i], "sum", tp=ty[3])
     up(ty[1])
     down(part.at[1])
-    b_right = cm.start(part.at[1, 128:256], fin.at[1], tp=ty[1])
+    direct = cm.slot()
+    cm.start(part.at[1, 128:256], fin.at[1], direct, "sum", tp=ty[1])
     up(ty[3])
     down(part.at[2])
-    a_left = cm.start(part.at[2, 0:128], fin.at[2], tp=ty[3])
+    cm.start(part.at[2, 0:128], fin.at[2], direct, "sum", tp=ty[3])
 
     def joined(which, rows, side):
         base = 0 if side.start == 0 else D // 2
@@ -502,21 +548,19 @@
             total = part[1 + which, rows, cols].astype(F32) + rin[which, :, cols].astype(F32)
             part[1 + which, rows, cols] = total.astype(BF16)
 
-    a_right, b_left = [], []
+    f_both = []
     for i, side in enumerate(sides):
-        s_right[i].wait_recv()
+        s_both[i].wait_recv()
+        f_both.append(cm.slot())
         joined(0, slice(0, 128), side)
-        a_right.append(cm.start(part.at[1, 0:128, side], fin.at[0, :, side], tp=ty[1]))
-        s_left[i].wait_recv()
+        cm.start(part.at[1, 0:128, side], fin.at[0, :, side], f_both[i], "sum", tp=ty[1])
         joined(1, slice(128, 256), side)
-        b_left.append(cm.start(part.at[2, 128:256, side], fin.at[3, :, side], tp=ty[3]))
+        cm.start(part.at[2, 128:256, side], fin.at[3, :, side], f_both[i], "sum", tp=ty[3])
     up(t)
     down(own)
-    b_right.wait_recv()
-    a_left.wait_recv()
+    direct.wait_recv()
     for i, side in enumerate(sides):
-        a_right[i].wait_recv()
-        b_left[i].wait_recv()
+        f_both[i].wait_recv()
 
         @pl.loop(4 * i, 4 * i + 4)
         def _(n):
@@ -527,8 +571,7 @@
                 ffn = own[rows, cols] + fin[k, :, cols].astype(F32) + fin[2 + k, :, cols].astype(F32)
                 out_ref[rows, cols] = (res[mrows, cols].astype(F32) + ffn).astype(BF16)
 
-    for copy in cm.all:
-        copy.wait_send()
+    cm.sent()
 
 
 def shards(
@@ -545,20 +588,17 @@
     conv_value,
     w_down,
 ):
-    offset = lax.axis_index("sp") * ROWS
     inverse = 1.0 / THETA ** (jnp.arange(0, HD, 2, dtype=F32) / HD)
-    within = jnp.arange(WINDOW, dtype=jnp.int32)
-    starts = offset + (jnp.arange(16, dtype=jnp.int32) - 1) * WINDOW
-    positions = jnp.concatenate([within, starts]).astype(F32)
-    angle = positions[:, None] * jnp.tile(inverse, 4)[None, :]
     vmem = pl.BlockSpec(memory_space=pltpu.VMEM)
     hbm = pl.BlockSpec(memory_space=pl.ANY)
     return pl.pallas_call(
         layer,
         out_shape=jax.ShapeDtypeStruct((CH, D), BF16),
-        in_specs=[pl.BlockSpec(memory_space=pltpu.SMEM)] + [vmem] * 2 + [hbm] * 11,
+        in_specs=[pl.BlockSpec(memory_space=pltpu.SMEM)] + [vmem] + [hbm] * 11,
         out_specs=vmem,
         scratch_shapes=[
+            pltpu.VMEM((WINDOW + 16, 128), F32),
+            pltpu.VMEM((WINDOW + 16, 128), F32),
             pltpu.VMEM((ROWS, QC), BF16),
             pltpu.VMEM((1, D), F32),
             pltpu.VMEM((3, FL), BF16),
@@ -583,8 +623,8 @@
             pltpu.VMEM((CH, D), F32),
             pltpu.VMEM((2, 128, D), BF16),
             pltpu.VMEM((4, 128, D), BF16),
-            pltpu.SemaphoreType.DMA((NSEM,)),
-            pltpu.SemaphoreType.DMA((NSEM,)),
+            pltpu.SemaphoreType.DMA((NSEND,)),
+            pltpu.SemaphoreType.DMA((NRECV,)),
             pltpu.SemaphoreType.DMA((NLOC,)),
         ],
         compiler_params=pltpu.CompilerParams(
@@ -593,8 +633,7 @@
         name="layer",
     )(
         sink,
-        jnp.cos(angle),
-        jnp.sin(angle),
+        jnp.tile(inverse, 4).reshape(1, 128),
         query,
         norm_gain.reshape(1, D),
         conv_gate,

time: 103 us -> 101 us (0.981)
  Pallas kernels: 99 us -> 97.9 us
    pallas_call x1, Pallas kernels: 99 us -> 97.9 us  [shards(): pl.pallas_call(layer, out_shape=jax.ShapeDtypeStruct((CH, D), BF16), in_s...]
where the time goes in v3:
time: 101 us
  Pallas kernels  97.9 us (97%)
  local copies, waits for them, and re-layouts  2.91 us (3%)
    pallas_call x1, Pallas kernels, shards(): pl.pallas_call(layer, out_shape=jax.ShapeDtypeStruct((CH, D), BF16), in_s...  97.9 us
    unnamed x1, local copies, waits for them, and re-layouts  2.3 us

profile of v3, /device:TPU:1, one launch (start us, length us, event | category | flops | bytes accessed | tf_op | source)
XLA Modules:
  0.0 100.8 jit_solution(17766828782778012598)
XLA Ops:
  0.0 0.6 reshape_tile.3.inverse_ref
  0.6 97.9 %layer.1 = bf16[256,2048]{1,0:T(8,128)(2,1)} custom-call(f32[4]{0:T(128)} %sink_ref.1, f32[1,128]{1,0:T(1,128)} %reshape_tile.3.inverse_ref, bf16[1024,256]{1,0:T(8,128)(2,1)} %q_hbm.1, f32[1,2048]{1,0:T(1,128)} %bitcast.7, bf16[3,1024]{1,0:T(4,128)(2,1)} %tap_gate_hbm.1, bf16[3,1024]{1,0:T(4,128)(2,1)} %tap_value_hbm.1, bf16[64,1024]{1,0:T(8,128)(2,1)} %bitcast.4, ...), custom_call_target="tpu_custom_call" | custom-call | tf_op jit(solution)/shard_map/layer/pallas_call | solution.py:594
  98.5 2.3 %copy.14 = bf16[256,2048]{1,0:T(8,128)(2,1)} copy(bf16[256,2048]{1,0:T(8,128)(2,1)} %layer.1) | data formatting | bytes 2097152
  (2 shorter events, 0.0 us)

commit v4 on v3

--- a/solution.py
+++ b/solution.py
@@ -22,7 +22,7 @@
 HALO = 16
 NSEND = 6
 NRECV = 64
-NLOC = 12
+NLOC = 14
 NT = (((1,), (1,)), ((), ()))
 F32 = jnp.float32
 BF16 = jnp.bfloat16
@@ -107,7 +107,7 @@
     g_hbm,
     v_hbm,
     d_hbm,
-    out_ref,
+    out_hbm,
     cos_ref,
     sin_ref,
     q_ref,
@@ -502,28 +502,28 @@
     g_round(3)
     e_both = cm.slot()
     cm.start(nrm.at[pl.ds(HALO, HALO)], edge.at[1], e_both, sp=behind)
+    middle(1)
+    cm.start(nrm.at[pl.ds(ROWS, HALO)], edge.at[0], e_both, sp=ahead)
     fd.pass_on(3)
     fd.pass_on(-3)
     fd.pass_on(-4)
-    middle(1)
-    cm.start(nrm.at[pl.ds(ROWS, HALO)], edge.at[0], e_both, sp=ahead)
     for o in (3, -3, -4):
         fv.last(o)
-    for o in (0, 1, -1, 2, -2):
-        fd.last(o)
     middle(2)
     g_round(4)
-    for o in (3, -3, -4):
-        fd.share(o)
+    for o in (0, 1, -1, 2, -2):
         fd.last(o)
     fv.arrived()
     g_push.wait_recv()
     e_both.wait_recv()
     nrm[0:HALO, :] = jnp.where(s > 0, edge[0].astype(F32), 0.0).astype(BF16)
     nrm[HALO + ROWS :, :] = jnp.where(s < nsp - 1, edge[1].astype(F32), 0.0).astype(BF16)
+    for o in (3, -3, -4):
+        fd.share(o)
+        fd.last(o)
+    up(ty[2])
     fd.arrived()
     turn_down()
-    up(ty[2])
     sides = (slice(0, D // 2), slice(D // 2, D))
     s_both = []
     for i, side in enumerate(sides):
@@ -559,6 +559,7 @@
     up(t)
     down(own)
     direct.wait_recv()
+    written = []
     for i, side in enumerate(sides):
         f_both[i].wait_recv()
 
@@ -569,9 +570,13 @@
                 rows = slice(k * 128, k * 128 + 128)
                 mrows = pl.ds(pl.multiple_of(t * CH + k * 128, 128), 128)
                 ffn = own[rows, cols] + fin[k, :, cols].astype(F32) + fin[2 + k, :, cols].astype(F32)
-                out_ref[rows, cols] = (res[mrows, cols].astype(F32) + ffn).astype(BF16)
+                own[rows, cols] = res[mrows, cols].astype(F32) + ffn
+
+        written.append(cm.here(own.at[:, side], out_hbm.at[:, side]))
 
     cm.sent()
+    for copy in written:
+        copy.wait()
 
 
 def shards(
@@ -588,14 +593,15 @@
     conv_value,
     w_down,
 ):
-    inverse = 1.0 / THETA ** (jnp.arange(0, HD, 2, dtype=F32) / HD)
+    pair = (jnp.arange(128, dtype=jnp.int32) % (HD // 2) * 2).astype(F32)
+    inverse = 1.0 / THETA ** (pair / HD)
     vmem = pl.BlockSpec(memory_space=pltpu.VMEM)
     hbm = pl.BlockSpec(memory_space=pl.ANY)
-    return pl.pallas_call(
+    total = pl.pallas_call(
         layer,
-        out_shape=jax.ShapeDtypeStruct((CH, D), BF16),
+        out_shape=jax.ShapeDtypeStruct((CH, D), F32),
         in_specs=[pl.BlockSpec(memory_space=pltpu.SMEM)] + [vmem] + [hbm] * 11,
-        out_specs=vmem,
+        out_specs=hbm,
         scratch_shapes=[
             pltpu.VMEM((WINDOW + 16, 128), F32),
             pltpu.VMEM((WINDOW + 16, 128), F32),
@@ -633,7 +639,7 @@
         name="layer",
     )(
         sink,
-        jnp.tile(inverse, 4).reshape(1, 128),
+        inverse.reshape(1, 128),
         query,
         norm_gain.reshape(1, D),
         conv_gate,
@@ -646,6 +652,7 @@
         w_value,
         w_down.T,
     )
+    return total.astype(BF16)
 
 
 def solution(mesh):

time: 101 us -> 101 us (level)
  other arithmetic: 0.01 us -> 3.24 us
  local copies, waits for them, and re-layouts: 2.91 us -> 0 us
    convert_element_type x0 -> x1, other arithmetic: none -> 2.71 us  [shards(): return total.astype(BF16)]
    unnamed x1 -> x0, local copies, waits for them, and re-layouts: 2.3 us -> none
where the time goes in v4:
time: 101 us
  Pallas kernels  97.9 us (97%)
  other arithmetic  3.24 us (3%)
    pallas_call x1, Pallas kernels, shards(): pl.pallas_call(layer, out_shape=jax.ShapeDtypeStruct((CH, D), F32), in_sp...  97.9 us
    convert_element_type x1, other arithmetic, shards(): return total.astype(BF16)  2.71 us

profile of v4, /device:TPU:1, one launch (start us, length us, event | category | flops | bytes accessed | tf_op | source)
XLA Modules:
  0.0 101.2 jit_solution(14695058941180636049)
XLA Ops:
  0.0 0.5 fusion.4.inverse_ref
  0.5 97.9 %layer.1 = f32[256,2048]{1,0:T(8,128)} custom-call(f32[4]{0:T(128)} %sink_ref.1, f32[1,128]{1,0:T(1,128)} %fusion.4.inverse_ref, bf16[1024,256]{1,0:T(8,128)(2,1)} %q_hbm.1, f32[1,2048]{1,0:T(1,128)} %bitcast.7, bf16[3,1024]{1,0:T(4,128)(2,1)} %tap_gate_hbm.1, bf16[3,1024]{1,0:T(4,128)(2,1)} %tap_value_hbm.1, bf16[64,1024]{1,0:T(8,128)(2,1)} %bitcast.4, ...), custom_call_target="tpu_custom_call" | custom-call | tf_op jit(solution)/shard_map/layer/pallas_call | solution.py:600
  98.5 2.7 %convert_element_type.14 = bf16[256,2048]{1,0:T(8,128)(2,1)} convert(f32[256,2048]{1,0:T(8,128)} %layer.1) | non-fusion elementwise | flops 524288 | bytes 3145728 | tf_op jit(solution)/shard_map/convert_element_type | solution.py:655

commit v5 on v4

--- a/solution.py
+++ b/solution.py
@@ -132,6 +132,7 @@
     hid,
     part,
     own,
+    result,
     rin,
     fin,
     send,
@@ -570,9 +571,9 @@
                 rows = slice(k * 128, k * 128 + 128)
                 mrows = pl.ds(pl.multiple_of(t * CH + k * 128, 128), 128)
                 ffn = own[rows, cols] + fin[k, :, cols].astype(F32) + fin[2 + k, :, cols].astype(F32)
-                own[rows, cols] = res[mrows, cols].astype(F32) + ffn
-
-        written.append(cm.here(own.at[:, side], out_hbm.at[:, side]))
+                result[rows, cols] = (res[mrows, cols].astype(F32) + ffn).astype(BF16)
+
+        written.append(cm.here(result.at[:, side], out_hbm.at[:, side]))
 
     cm.sent()
     for copy in written:
@@ -597,9 +598,9 @@
     inverse = 1.0 / THETA ** (pair / HD)
     vmem = pl.BlockSpec(memory_space=pltpu.VMEM)
     hbm = pl.BlockSpec(memory_space=pl.ANY)
-    total = pl.pallas_call(
+    return pl.pallas_call(
         layer,
-        out_shape=jax.ShapeDtypeStruct((CH, D), F32),
+        out_shape=jax.ShapeDtypeStruct((CH, D), BF16),
         in_specs=[pl.BlockSpec(memory_space=pltpu.SMEM)] + [vmem] + [hbm] * 11,
         out_specs=hbm,
         scratch_shapes=[
@@ -627,6 +628,7 @@
             pltpu.VMEM((CH, FL), BF16),
             pltpu.VMEM((3, CH, D), BF16),
             pltpu.VMEM((CH, D), F32),
+            pltpu.VMEM((CH, D), BF16),
             pltpu.VMEM((2, 128, D), BF16),
             pltpu.VMEM((4, 128, D), BF16),
             pltpu.SemaphoreType.DMA((NSEND,)),
@@ -652,7 +654,6 @@
         w_value,
         w_down.T,
     )
-    return total.astype(BF16)
 
 
 def solution(mesh):

time: 101 us -> 101 us (level)
  other arithmetic: 3.24 us -> 0.52 us
  local copies, waits for them, and re-layouts: 0 us -> 2.3 us
    convert_element_type x1 -> x0, other arithmetic: 2.71 us -> none  [shards(): return total.astype(BF16)]
    unnamed x0 -> x1, local copies, waits for them, and re-layouts: none -> 2.3 us
where the time goes in v5:
time: 101 us
  Pallas kernels  97.7 us (97%)
  local copies, waits for them, and re-layouts  2.3 us (2%)
    pallas_call x1, Pallas kernels, shards(): pl.pallas_call(layer, out_shape=jax.ShapeDtypeStruct((CH, D), BF16), in_s...  97.7 us
    unnamed x1, local copies, waits for them, and re-layouts  2.3 us

profile of v5, /device:TPU:1, one launch (start us, length us, event | category | flops | bytes accessed | tf_op | source)
XLA Modules:
  0.0 100.6 jit_solution(10847104209522425950)
XLA Ops:
  0.0 0.5 fusion.4.inverse_ref
  0.5 97.7 %layer.1 = bf16[256,2048]{1,0:T(8,128)(2,1)} custom-call(f32[4]{0:T(128)} %sink_ref.1, f32[1,128]{1,0:T(1,128)} %fusion.4.inverse_ref, bf16[1024,256]{1,0:T(8,128)(2,1)} %q_hbm.1, f32[1,2048]{1,0:T(1,128)} %bitcast.7, bf16[3,1024]{1,0:T(4,128)(2,1)} %tap_gate_hbm.1, bf16[3,1024]{1,0:T(4,128)(2,1)} %tap_value_hbm.1, bf16[64,1024]{1,0:T(8,128)(2,1)} %bitcast.4, ...), custom_call_target="tpu_custom_call" | custom-call | tf_op jit(solution)/shard_map/layer/pallas_call | solution.py:601
  98.3 2.3 %copy.14 = bf16[256,2048]{1,0:T(8,128)(2,1)} copy(bf16[256,2048]{1,0:T(8,128)(2,1)} %layer.1) | data formatting | bytes 2097152
